TPU v7x, 32 devices: a whole 2x2x4 slice. The times are simulated.
32 devices in a mesh: ep: 8 (over z, y), tp: 4 (over x, core).
Axes of the slice: x: 2, y: 2, z: 4, core: 2. Of those that a mesh axis runs over, the one named last changes fastest.
Arguments:
- tokens: bfloat16 [1024, 2048], P('ep'), may hold values from -6 to 6
- norm_gain: float32 [2048], replicated, may hold values from 0.1 to 1.9
- routes: int32 [1024, 2], P('ep'), may hold values from 0 to 7, all different within a row; in each aligned block of 128 rows (0 to 127, 128 to 255, ...) at most 48 rows name the same one
- group_prob: float32 [1024], P('ep'), may hold values from 0.2 to 1
- expert_logits: float32 [1024, 2], P('ep'), may hold values from -6 to 6
- gate_weight: bfloat16 [8, 2048, 384], P('ep', None, 'tp'), may hold values from -0.125 to 0.125
- up_weight: bfloat16 [8, 2048, 384], P('ep', None, 'tp'), may hold values from -0.125 to 0.125
- down_matrix: bfloat16 [8, 384, 2048], P('ep', 'tp'), may hold values from -0.3125 to 0.3125
Outputs:
- combined: bfloat16 [1024, 2048], P('ep', 'tp')
Inputs may be any that keep to these rules, and one draw needn't show every extreme that they name: `routes`: each row names 2 different experts. Among the 128 tokens of one index of ep at most 48 rows name one expert, and in every draw some expert is named by exactly 48 of them.
All inputs are finite; a program needn't handle non-finite values.
Results may differ from a plain program's by a relative error of at most 0.013.
Values may be sent and summed in bfloat16 or wider, within the bound.
A program may use at most 64 MiB of HBM per device.

v0:
```python
import functools

import jax
import jax.numpy as jnp
from jax import lax
from jax.experimental import pallas as pl
from jax.experimental.pallas import tpu as pltpu
from jax.sharding import PartitionSpec as P


def hidden_part(buffer, gate_weight, up_weight):
    local_count = gate_weight.shape[0]
    grouped = buffer.reshape(
        buffer.shape[0] // local_count, local_count, buffer.shape[1], buffer.shape[2]
    )
    gate_proj = jnp.einsum(
        "sknd,kdf->sknf", grouped, gate_weight, preferred_element_type=jnp.float32
    )
    up_proj = jnp.einsum("sknd,kdf->sknf", grouped, up_weight, preferred_element_type=jnp.float32)
    hidden_state = (jax.nn.silu(gate_proj) * up_proj).astype(jnp.bfloat16)
    return hidden_state.reshape(buffer.shape[0], buffer.shape[1], hidden_state.shape[3])


def down_blocks(hidden_full, down_cols, block_count):
    local_count = down_cols.shape[0]
    width = hidden_full.shape[2] // block_count
    grouped = hidden_full.reshape(
        hidden_full.shape[0] // local_count, local_count, hidden_full.shape[1], block_count, width
    )
    columns = down_cols.reshape(local_count, block_count, width, down_cols.shape[2])
    block_list = jnp.einsum(
        "sknrf,krfd->sknrd", grouped, columns, preferred_element_type=jnp.float32
    ).astype(jnp.bfloat16)
    summed = jnp.sum(block_list.astype(jnp.float32), 3).astype(jnp.bfloat16)
    return summed.reshape(hidden_full.shape[0], hidden_full.shape[1], down_cols.shape[2])


def body(tokens, norm_gain, routes, group_prob, expert_logits, gate_weight, up_weight, down_matrix):
    tok_rows, model_width = tokens.shape
    top_count = routes.shape[1]
    experts = gate_weight.shape[0] * lax.axis_size("ep")
    capacity = 3 * top_count * tok_rows // (2 * experts)
    block_count = lax.axis_size("tp")
    down_cols = lax.all_to_all(down_matrix, "tp", split_axis=2, concat_axis=1, tiled=True)
    values = tokens.astype(jnp.float32)
    normed = (
        values * lax.rsqrt(jnp.mean(values * values, -1, keepdims=True) + 1e-06) * norm_gain
    ).astype(jnp.bfloat16)
    flat_ids = routes.reshape(-1)
    onehot = (flat_ids[:, None] == jnp.arange(experts, dtype=jnp.int32)[None, :]).astype(jnp.int32)
    earlier = jnp.cumsum(onehot, 0) - onehot
    slot_index = jnp.sum(earlier * onehot, 1)
    target = flat_ids * capacity + slot_index
    owners = jnp.arange(tok_rows * top_count, dtype=jnp.int32) // top_count
    outgoing = (
        jnp.zeros((experts * capacity, model_width), jnp.bfloat16).at[target].set(normed[owners])
    )
    outgoing = outgoing.reshape(experts, capacity, model_width)
    hidden_state = hidden_part(
        lax.all_to_all(outgoing, "ep", split_axis=0, concat_axis=0, tiled=True),
        gate_weight,
        up_weight,
    )
    hidden_full = lax.all_gather(hidden_state, "tp", axis=2, tiled=True)
    summed = down_blocks(hidden_full, down_cols, block_count)
    returned = lax.all_to_all(summed, "ep", split_axis=0, concat_axis=0, tiled=True)
    flat_back = returned.reshape(experts * capacity, returned.shape[2])
    weights = group_prob[:, None] * jax.nn.softmax(expert_logits, axis=-1)
    picked = flat_back[target].reshape(tok_rows, top_count, flat_back.shape[1]).astype(jnp.float32)
    combined = jnp.sum(picked * weights[:, :, None], 1).astype(jnp.bfloat16)
    return combined


MESH = pl.DeviceIdType.MESH
F32, BF16 = jnp.float32, jnp.bfloat16


def round_up(value, step):
    return -(-value // step) * step


def toggled(index, mask):
    bit = 1
    result = index
    while bit <= mask:
        if mask & bit:
            result = result + bit * (1 - 2 * ((index // bit) % 2))
        bit *= 2
    return result


def expert_kernel(
    n_ep, n_tp, capacity, width,
    tokens_hbm, gain_hbm, routes_hbm, prob_hbm, logits_hbm, gate_ref, up_ref, down_ref,
    out_ref,
    tokens_ref, gain_ref, routes_ref, prob_ref, logits_ref, load_sem, normed, select, weigh, outgoing, arrived, gate_up, down_cols, hidden, result, returned,
    send_disp, recv_disp, send_core, recv_core, send_side, recv_side, send_relay, recv_relay,
    send_down, recv_down, send_hid, recv_hid, send_back, recv_back,
):
    loads = [
        pltpu.make_async_copy(source, target, load_sem.at[i])
        for i, (source, target) in enumerate((
            (routes_hbm, routes_ref), (tokens_hbm, tokens_ref), (gain_hbm, gain_ref),
            (prob_hbm, prob_ref), (logits_hbm, logits_ref),
        ))
    ]
    for load in loads:
        load.start()
    rows, model = tokens_ref.shape
    quarter = model // n_tp
    fpad = gate_up.shape[0] // 2
    n_hi = n_tp // 2
    slots = n_ep * capacity
    e = lax.axis_index("ep")
    t = lax.axis_index("tp")
    partner = t + 1 - 2 * (t % 2)

    def over(index, h):
        return (index + 2 * h) % n_tp

    def back(index, h):
        return (index + n_tp - 2 * h) % n_tp

    barrier = pltpu.get_barrier_semaphore()
    for r in range(1, n_ep):
        pl.semaphore_signal(barrier, inc=1, device_id={"ep": toggled(e, r), "tp": t}, device_id_type=MESH)
    for j in range(1, n_tp):
        pl.semaphore_signal(barrier, inc=1, device_id={"ep": e, "tp": (t + j) % n_tp}, device_id_type=MESH)

    fetch_gate = pltpu.make_async_copy(gate_ref, gate_up.at[pl.ds(0, width)], load_sem.at[5])
    fetch_up = pltpu.make_async_copy(up_ref, gate_up.at[pl.ds(fpad, width)], load_sem.at[6])
    fetch_down = pltpu.make_async_copy(
        down_ref.at[:, pl.ds(pl.multiple_of(t * quarter, quarter), quarter)],
        down_cols.at[t, pl.ds(0, width)], load_sem.at[7])
    fetches = [fetch_gate, fetch_up, fetch_down]
    for fetch in fetches:
        fetch.start()
    for load in loads:
        load.wait()

    first, second = routes_ref[0:1, :], routes_ref[1:2, :]
    lanes = round_up(n_ep, 16)
    expert_row = lax.broadcasted_iota(jnp.int32, (lanes, rows), 0)
    hit0 = (expert_row == first).astype(F32)
    hit1 = (expert_row == second).astype(F32)
    before = (
        lax.broadcasted_iota(jnp.int32, (rows, rows), 0) < lax.broadcasted_iota(jnp.int32, (rows, rows), 1)
    ).astype(F32).astype(BF16)
    earlier = jnp.dot((hit0 + hit1).astype(BF16), before, preferred_element_type=F32)
    slot0 = jnp.sum(earlier * hit0, 0, keepdims=True)
    slot1 = jnp.sum(earlier * hit1, 0, keepdims=True)
    place0 = first * capacity + slot0.astype(jnp.int32)
    place1 = second * capacity + slot1.astype(jnp.int32)
    slot_row = lax.broadcasted_iota(jnp.int32, (slots, rows), 0)
    at0, at1 = slot_row == place0, slot_row == place1
    select[...] = (at0.astype(F32) + at1.astype(F32)).astype(BF16)

    values = tokens_ref[...].astype(F32)
    scale = lax.rsqrt(jnp.mean(values * values, -1, keepdims=True) + 1e-06)
    normed[...] = (values * scale * gain_ref[...]).astype(BF16)

    for h in range(n_hi):
        part = normed[:, pl.ds(pl.multiple_of(back(t, h) * quarter, quarter), quarter)]
        packed = jnp.dot(select[...], part, preferred_element_type=F32).astype(BF16)
        outgoing[h] = packed.reshape(n_ep, capacity, quarter)

    pl.semaphore_wait(barrier, n_ep - 1 + n_tp - 1)

    def disp(r, h=0):
        peer = toggled(e, r)
        origin = back(t, h)
        return pltpu.make_async_remote_copy(
            src_ref=outgoing.at[h, peer], dst_ref=arrived.at[r, origin],
            send_sem=send_disp.at[r, h], recv_sem=recv_disp.at[r, h],
            device_id={"ep": peer, "tp": t}, device_id_type=MESH)

    def core(r):
        return pltpu.make_async_remote_copy(
            src_ref=arrived.at[r, t], dst_ref=arrived.at[r, t], send_sem=send_core.at[r], recv_sem=recv_core.at[r],
            device_id={"ep": e, "tp": partner}, device_id_type=MESH)

    def side(r, h):
        return pltpu.make_async_remote_copy(
            src_ref=arrived.at[r, t], dst_ref=arrived.at[r, t], send_sem=send_side.at[r, h], recv_sem=recv_side.at[r, h],
            device_id={"ep": e, "tp": over(t, h)}, device_id_type=MESH)

    def relay(r, h):
        origin = back(t, h)
        return pltpu.make_async_remote_copy(
            src_ref=arrived.at[r, origin], dst_ref=arrived.at[r, origin],
            send_sem=send_relay.at[r, h], recv_sem=recv_relay.at[r, h],
            device_id={"ep": e, "tp": partner}, device_id_type=MESH)

    def down(j):
        peer = (t + j) % n_tp
        return pltpu.make_async_remote_copy(
            src_ref=down_ref.at[:, pl.ds(pl.multiple_of(peer * quarter, quarter), quarter)],
            dst_ref=down_cols.at[t, pl.ds(0, width)], send_sem=send_down.at[j], recv_sem=recv_down.at[j],
            device_id={"ep": e, "tp": peer}, device_id_type=MESH)

    def hid(p, j):
        return pltpu.make_async_remote_copy(
            src_ref=hidden.at[p, t], dst_ref=hidden.at[p, t], send_sem=send_hid.at[p, j], recv_sem=recv_hid.at[p, j],
            device_id={"ep": e, "tp": (t + j) % n_tp}, device_id_type=MESH)

    def home(r):
        return pltpu.make_async_remote_copy(
            src_ref=result.at[r], dst_ref=returned.at[e], send_sem=send_back.at[r], recv_sem=recv_back.at[r],
            device_id={"ep": toggled(e, r), "tp": t}, device_id_type=MESH)

    def landed(ref, sem):
        pltpu.make_async_copy(ref, ref, sem).wait()

    near = range(1, n_ep // 2)
    far = range(max(1, n_ep // 2), n_ep)
    for r in near:
        for h in range(n_hi):
            disp(r, h).start()
    for r in far:
        disp(r).start()
    for j in range(1, n_tp):
        down(j).start()

    if fpad > width:
        gate_up[width:fpad] = jnp.zeros((fpad - width, model), BF16)
        gate_up[fpad + width:] = jnp.zeros((fpad - width, model), BF16)
        down_cols[:, width:fpad] = jnp.zeros((n_tp, fpad - width, quarter), BF16)

    logit0, logit1 = logits_ref[0:1, :], logits_ref[1:2, :]
    top = jnp.maximum(logit0, logit1)
    exp0, exp1 = jnp.exp(logit0 - top), jnp.exp(logit1 - top)
    share = prob_ref[...] / (exp0 + exp1)
    weight = (jnp.where(at0, share * exp0, 0.0) + jnp.where(at1, share * exp1, 0.0)).T
    high = weight.astype(BF16)
    weigh[0] = high
    weigh[1] = (weight - high.astype(F32)).astype(BF16)

    def product(left, right):
        return lax.dot_general(left, right, (((1,), (1,)), ((), ())), preferred_element_type=F32)

    def take(r):
        landed(arrived.at[r, t], recv_disp.at[r, 0])
        if r in far:
            for h in range(1, n_hi):
                side(r, h).start()
        core(r).start()
        if r in near:
            for h in range(1, n_hi):
                landed(arrived.at[r, back(t, h)], recv_disp.at[r, h])
                relay(r, h).start()

    def pass_on(r):
        for h in range(1, n_hi):
            landed(arrived.at[r, back(t, h)], recv_side.at[r, h])
            relay(r, h).start()

    def expand(p):
        for r in (2 * p, 2 * p + 1):
            if r:
                landed(arrived.at[r, partner], recv_core.at[r])
                for h in range(1, n_hi):
                    landed(arrived.at[r, back(partner, h)], recv_relay.at[r, h])
            else:
                own = select[pl.ds(pl.multiple_of(e * capacity, capacity), capacity)]
                for q in range(n_tp):
                    block = jnp.dot(own, normed[:, q * quarter:(q + 1) * quarter], preferred_element_type=F32)
                    arrived[0, q] = block.astype(BF16)
        acc = jnp.zeros((2 * capacity, 2 * fpad), F32)
        for q in range(n_tp):
            block = arrived[2 * p:2 * p + 2, q].reshape(2 * capacity, quarter)
            acc = acc + product(block, gate_up[:, q * quarter:(q + 1) * quarter])
        gate, up = acc[:, :fpad], acc[:, fpad:]
        hidden[p, t] = (gate / (1.0 + jnp.exp(-gate)) * up).astype(BF16)
        for j in range(1, n_tp):
            hid(p, j).start()

    def contract(p):
        for j in range(1, n_tp):
            landed(hidden.at[p, (t + n_tp - j) % n_tp], recv_hid.at[p, j])
        acc = jnp.zeros((2 * capacity, quarter), F32)
        for q in range(n_tp):
            acc = acc + jnp.dot(hidden[p, q], down_cols[q], preferred_element_type=F32)
        for i in range(2):
            r = 2 * p + i
            block = acc[i * capacity:(i + 1) * capacity].astype(BF16)
            if r:
                result[r] = block
                home(r).start()
            else:
                returned[e] = block

    for fetch in fetches:
        fetch.wait()
    pairs = n_ep // 2
    todo = []
    for p in range(pairs):
        rounds = [r for r in (2 * p, 2 * p + 1) if r]
        todo.append((3 * p, take, rounds))
        todo.append((3 * p + 3, pass_on, [r for r in rounds if r in far]))
        todo.append((3 * p + 4 if rounds[0] in far else 3 * p + 2, expand, [p]))
        todo.append((3 * p + 8 if rounds[0] in far else 3 * p + 6, contract, [p]))
    todo.sort(key=lambda entry: entry[0])
    waited = False
    for _, stage, items in todo:
        if stage is contract and not waited:
            waited = True
            for j in range(1, n_tp):
                landed(down_cols.at[(t + n_tp - j) % n_tp, pl.ds(0, width)], recv_down.at[j])
        for item in items:
            stage(item)

    for r in range(1, n_ep):
        landed(returned.at[toggled(e, r)], recv_back.at[r])
    back_rows = returned[...].reshape(slots, quarter)
    total = jnp.dot(weigh[0], back_rows, preferred_element_type=F32)
    total = total + jnp.dot(weigh[1], back_rows, preferred_element_type=F32)
    out_ref[...] = total.astype(BF16)

    for r in range(1, n_ep):
        disp(r).wait_send()
        core(r).wait_send()
        home(r).wait_send()
        for h in range(1, n_hi):
            if r in near:
                disp(r, h).wait_send()
            else:
                side(r, h).wait_send()
            relay(r, h).wait_send()
    for j in range(1, n_tp):
        down(j).wait_send()
        for p in range(pairs):
            hid(p, j).wait_send()


def fused_body(tokens, norm_gain, routes, group_prob, expert_logits, gate_weight, up_weight, down_matrix):
    n_ep, n_tp = lax.axis_size("ep"), lax.axis_size("tp")
    rows, model = tokens.shape
    capacity = 3 * routes.shape[1] * rows // (2 * n_ep)
    width = gate_weight.shape[2]
    fpad = round_up(width, 128)
    quarter = model // n_tp
    n_hi = n_tp // 2
    sem = pltpu.SemaphoreType.DMA
    vmem = pl.BlockSpec(memory_space=pltpu.VMEM)
    return pl.pallas_call(
        functools.partial(expert_kernel, n_ep, n_tp, capacity, width),
        out_shape=jax.ShapeDtypeStruct((rows, quarter), BF16),
        in_specs=[pl.BlockSpec(memory_space=pl.ANY)] * 8,
        out_specs=vmem,
        scratch_shapes=[
            pltpu.VMEM((rows, model), BF16),
            pltpu.VMEM((1, model), F32),
            pltpu.VMEM((2, rows), jnp.int32),
            pltpu.VMEM((1, rows), F32),
            pltpu.VMEM((2, rows), F32),
            sem((8,)),
            pltpu.VMEM((rows, model), BF16),
            pltpu.VMEM((n_ep * capacity, rows), BF16),
            pltpu.VMEM((2, rows, n_ep * capacity), BF16),
            pltpu.VMEM((n_hi, n_ep, capacity, quarter), BF16),
            pltpu.VMEM((n_ep, n_tp, capacity, quarter), BF16),
            pltpu.VMEM((2 * fpad, model), BF16),
            pltpu.VMEM((n_tp, fpad, quarter), BF16),
            pltpu.VMEM((n_ep // 2, n_tp, 2 * capacity, fpad), BF16),
            pltpu.VMEM((n_ep, capacity, quarter), BF16),
            pltpu.VMEM((n_ep, capacity, quarter), BF16),
            sem((n_ep, n_hi)), sem((n_ep, n_hi)),
            sem((n_ep,)), sem((n_ep,)),
            sem((n_ep, n_hi)), sem((n_ep, n_hi)),
            sem((n_ep, n_hi)), sem((n_ep, n_hi)),
            sem((n_tp,)), sem((n_tp,)),
            sem((n_ep, n_tp)), sem((n_ep, n_tp)),
            sem((n_ep,)), sem((n_ep,)),
        ],
        compiler_params=pltpu.CompilerParams(collective_id=0, has_side_effects=True),
    )(
        tokens, norm_gain.reshape(1, model), routes.T, group_prob.reshape(1, rows), expert_logits.T,
        gate_weight.reshape(model, width).T, up_weight.reshape(model, width).T, down_matrix.reshape(width, model),
    )


def fits_kernel(n_ep, n_tp, rows, experts, top, model):
    capacity = 3 * top * rows // (2 * experts)
    return (
        experts == n_ep and top == 2 and n_ep & (n_ep - 1) == 0 and n_ep <= 16 and n_tp % 2 == 0
        and capacity % 16 == 0 and rows % 128 == 0 and model % (128 * n_tp) == 0
    )


def solution(mesh):
    n_ep, n_tp = mesh.shape["ep"], mesh.shape["tp"]

    def chosen(*arrays):
        rows, model = arrays[0].shape
        fits = fits_kernel(n_ep, n_tp, rows, arrays[5].shape[0] * n_ep, arrays[2].shape[1], model)
        return (fused_body if fits else body)(*arrays)

    return jax.shard_map(
        chosen,
        mesh=mesh,
        in_specs=(
            P("ep", None),
            P(),
            P("ep", None),
            P("ep"),
            P("ep", None),
            P("ep", None, "tp"),
            P("ep", None, "tp"),
            P("ep", "tp", None),
        ),
        out_specs=P("ep", "tp"),
        check_vma=False,
    )
```

profile of v0, /device:TPU:0, one launch (start us, length us, event | category | flops | bytes accessed | tf_op | source)
XLA Modules:
  0.0 39.4 jit_solution(16172908359219256471)
XLA Ops:
  0.0 37.9 %shard_map.82 = bf16[128,512]{1,0:T(8,128)(2,1)} custom-call(bf16[128,2048]{1,0:T(8,128)(2,1)} %tokens_hbm.1, f32[1,2048]{1,0:T(1,128)} %bitcast.14, s32[2,128]{1,0:T(2,128)} %bitcast.15, f32[1,128]{1,0:T(1,128)} %bitcast.17, f32[2,128]{1,0:T(2,128)} %bitcast.16, bf16[96,2048]{1,0:T(8,128)(2,1)} %bitcast.11, bf16[96,2048]{1,0:T(8,128)(2,1)} %bitcast.12, ...), custom_call_target="tpu_custom_call" | custom-call | tf_op jit(solution)/shard_map/pallas_call | solution.py:345
  37.9 1.6 %copy.10 = bf16[128,512]{1,0:T(8,128)(2,1)} copy(bf16[128,512]{1,0:T(8,128)(2,1)} %shard_map.82) | data formatting | bytes 262144
where the time goes:
time: 39.6 us; the launch traced here: 39.4 us
  Pallas kernels  37.9 us (96%)
  local copies, waits for them, and re-layouts  1.57 us (4%)
    pallas_call x1, Pallas kernels, fused_body(): pl.pallas_call(functools.partial(expert_kernel, n_ep, n_tp, capacity, wid...  37.9 us
    unnamed x1, local copies, waits for them, and re-layouts  1.57 us

commit v1 on v0

--- a/solution.py
+++ b/solution.py
@@ -372,11 +372,11 @@
             sem((n_ep, n_tp)), sem((n_ep, n_tp)),
             sem((n_ep,)), sem((n_ep,)),
         ],
-        compiler_params=pltpu.CompilerParams(collective_id=0, has_side_effects=True),
-    )(
+        compiler_params=pltpu.CompilerParams(collective_id=0, has_side_effects=True, vmem_limit_bytes=32 * 1024 * 1024),
+    )(*[pltpu.with_memory_space_constraint(array, pltpu.HBM) for array in (
         tokens, norm_gain.reshape(1, model), routes.T, group_prob.reshape(1, rows), expert_logits.T,
         gate_weight.reshape(model, width).T, up_weight.reshape(model, width).T, down_matrix.reshape(width, model),
-    )
+    )])
 
 
 def fits_kernel(n_ep, n_tp, rows, experts, top, model):

time: 39.6 us -> 38 us (0.960)
  local copies, waits for them, and re-layouts: 1.57 us -> 0.66 us
  Pallas kernels: 37.9 us -> 37.2 us
    unnamed x1, local copies, waits for them, and re-layouts: 1.57 us -> 0.66 us
    pallas_call x1, Pallas kernels: 37.9 us -> 37.2 us  [fused_body(): pl.pallas_call(functools.partial(expert_kernel, n_ep, n_tp, capacity, wid...]
where the time goes in v1:
time: 38 us; the launch traced here: 37.9 us
  Pallas kernels  37.2 us (98%)
  local copies, waits for them, and re-layouts  0.66 us (2%)
    pallas_call x1, Pallas kernels, fused_body(): pl.pallas_call(functools.partial(expert_kernel, n_ep, n_tp, capacity, wid...  37.2 us

profile of v1, /device:TPU:0, one launch (start us, length us, event | category | flops | bytes accessed | tf_op | source)
XLA Modules:
  0.0 37.9 jit_solution(5946766982628449008)
XLA Ops:
  0.0 37.2 %shard_map.82 = bf16[128,512]{1,0:T(8,128)(2,1)S(1)} custom-call(bf16[128,2048]{1,0:T(8,128)(2,1)} %tokens_hbm.1, f32[1,2048]{1,0:T(1,128)} %bitcast.14, s32[2,128]{1,0:T(2,128)} %bitcast.15, f32[1,128]{1,0:T(1,128)} %bitcast.17, f32[2,128]{1,0:T(2,128)} %bitcast.16, bf16[96,2048]{1,0:T(8,128)(2,1)} %bitcast.11, bf16[96,2048]{1,0:T(8,128)(2,1)} %bitcast.12, ...), custom_call_target="tpu_custom_call" | custom-call | tf_op jit(solution)/shard_map/pallas_call | solution.py:345
  37.2 0.7 %copy.10 = bf16[128,512]{1,0:T(8,128)(2,1)} copy(bf16[128,512]{1,0:T(8,128)(2,1)S(1)} %shard_map.82) | data formatting | bytes 262144

commit v2 on v1

v2 whole, which is shorter than its diff:
```python
import functools

import jax
import jax.numpy as jnp
from jax import lax
from jax.experimental import pallas as pl
from jax.experimental.pallas import tpu as pltpu
from jax.sharding import PartitionSpec as P


def hidden_part(buffer, gate_weight, up_weight):
    local_count = gate_weight.shape[0]
    grouped = buffer.reshape(
        buffer.shape[0] // local_count, local_count, buffer.shape[1], buffer.shape[2]
    )
    gate_proj = jnp.einsum(
        "sknd,kdf->sknf", grouped, gate_weight, preferred_element_type=jnp.float32
    )
    up_proj = jnp.einsum("sknd,kdf->sknf", grouped, up_weight, preferred_element_type=jnp.float32)
    hidden_state = (jax.nn.silu(gate_proj) * up_proj).astype(jnp.bfloat16)
    return hidden_state.reshape(buffer.shape[0], buffer.shape[1], hidden_state.shape[3])


def down_blocks(hidden_full, down_cols, block_count):
    local_count = down_cols.shape[0]
    width = hidden_full.shape[2] // block_count
    grouped = hidden_full.reshape(
        hidden_full.shape[0] // local_count, local_count, hidden_full.shape[1], block_count, width
    )
    columns = down_cols.reshape(local_count, block_count, width, down_cols.shape[2])
    block_list = jnp.einsum(
        "sknrf,krfd->sknrd", grouped, columns, preferred_element_type=jnp.float32
    ).astype(jnp.bfloat16)
    summed = jnp.sum(block_list.astype(jnp.float32), 3).astype(jnp.bfloat16)
    return summed.reshape(hidden_full.shape[0], hidden_full.shape[1], down_cols.shape[2])


def body(tokens, norm_gain, routes, group_prob, expert_logits, gate_weight, up_weight, down_matrix):
    tok_rows, model_width = tokens.shape
    top_count = routes.shape[1]
    experts = gate_weight.shape[0] * lax.axis_size("ep")
    capacity = 3 * top_count * tok_rows // (2 * experts)
    block_count = lax.axis_size("tp")
    down_cols = lax.all_to_all(down_matrix, "tp", split_axis=2, concat_axis=1, tiled=True)
    values = tokens.astype(jnp.float32)
    normed = (
        values * lax.rsqrt(jnp.mean(values * values, -1, keepdims=True) + 1e-06) * norm_gain
    ).astype(jnp.bfloat16)
    flat_ids = routes.reshape(-1)
    onehot = (flat_ids[:, None] == jnp.arange(experts, dtype=jnp.int32)[None, :]).astype(jnp.int32)
    earlier = jnp.cumsum(onehot, 0) - onehot
    slot_index = jnp.sum(earlier * onehot, 1)
    target = flat_ids * capacity + slot_index
    owners = jnp.arange(tok_rows * top_count, dtype=jnp.int32) // top_count
    outgoing = (
        jnp.zeros((experts * capacity, model_width), jnp.bfloat16).at[target].set(normed[owners])
    )
    outgoing = outgoing.reshape(experts, capacity, model_width)
    hidden_state = hidden_part(
        lax.all_to_all(outgoing, "ep", split_axis=0, concat_axis=0, tiled=True),
        gate_weight,
        up_weight,
    )
    hidden_full = lax.all_gather(hidden_state, "tp", axis=2, tiled=True)
    summed = down_blocks(hidden_full, down_cols, block_count)
    returned = lax.all_to_all(summed, "ep", split_axis=0, concat_axis=0, tiled=True)
    flat_back = returned.reshape(experts * capacity, returned.shape[2])
    weights = group_prob[:, None] * jax.nn.softmax(expert_logits, axis=-1)
    picked = flat_back[target].reshape(tok_rows, top_count, flat_back.shape[1]).astype(jnp.float32)
    combined = jnp.sum(picked * weights[:, :, None], 1).astype(jnp.bfloat16)
    return combined


MESH = pl.DeviceIdType.MESH
F32, BF16 = jnp.float32, jnp.bfloat16


def round_up(value, step):
    return -(-value // step) * step


def SCOPE(name, run):
    run()


def flipped(index, bit):
    return bit * (1 - 2 * ((index // bit) % 2))


def toggled(index, mask):
    result, bit = index, 1
    while bit <= mask:
        if mask & bit:
            result = result + flipped(index, bit)
        bit *= 2
    return result


def expert_kernel(
    n_ep, capacity, width,
    tokens_hbm, gain_hbm, routes_hbm, prob_hbm, logits_hbm, gate_ref, up_ref, down_ref,
    out_ref,
    tokens_ref, gain_ref, routes_ref, prob_ref, logits_ref, normed, select, weigh, outgoing, arrived, gate_up, down_rows,
    hidden, result, returned,
    load_sem, send_disp, recv_disp, send_side, recv_side, send_hid, recv_hid, send_home, recv_home, send_weight, recv_weight,
):
    loads = [
        pltpu.make_async_copy(source, target, load_sem.at[i])
        for i, (source, target) in enumerate((
            (routes_hbm, routes_ref), (tokens_hbm, tokens_ref), (gain_hbm, gain_ref),
            (prob_hbm, prob_ref), (logits_hbm, logits_ref),
        ))
    ]
    for load in loads:
        load.start()
    rows, model = tokens_ref.shape
    half, quarter = model // 2, model // 4
    fpad = gate_up.shape[2]
    slots = n_ep * capacity
    e = lax.axis_index("ep")
    t = lax.axis_index("tp")
    x, c = t // 2, t % 2
    partner, across = t + 1 - 2 * c, (t + 2) % 4
    outer = 1 - ((e // 2) % 2 + (e // 4) % 2) % 2

    barrier = pltpu.get_barrier_semaphore()
    for r in range(n_ep):
        for mate in (t, partner):
            if r or mate is partner:
                pl.semaphore_signal(
                    barrier, inc=1, device_id={"ep": toggled(e, r), "tp": mate}, device_id_type=MESH)
    pl.semaphore_signal(barrier, inc=1, device_id={"ep": e, "tp": across}, device_id_type=MESH)

    columns = pl.ds(pl.multiple_of(x * half, half), half)
    fetches = [
        pltpu.make_async_copy(gate_ref, gate_up.at[0, c, pl.ds(0, width)], load_sem.at[5]),
        pltpu.make_async_copy(up_ref, gate_up.at[1, c, pl.ds(0, width)], load_sem.at[6]),
        pltpu.make_async_copy(down_ref.at[:, columns], down_rows.at[x, c, pl.ds(0, width)], load_sem.at[7]),
    ]
    for fetch in fetches:
        fetch.start()
    SCOPE("w_loads", lambda: [load.wait() for load in loads])

    first, second = routes_ref[0:1, :], routes_ref[1:2, :]
    lanes = round_up(n_ep, 16)
    expert_row = lax.broadcasted_iota(jnp.int32, (lanes, rows), 0)
    hit0 = (expert_row == first).astype(F32)
    hit1 = (expert_row == second).astype(F32)
    before = (
        lax.broadcasted_iota(jnp.int32, (rows, rows), 0) < lax.broadcasted_iota(jnp.int32, (rows, rows), 1)
    ).astype(F32).astype(BF16)
    earlier = jnp.dot((hit0 + hit1).astype(BF16), before, preferred_element_type=F32)
    slot0 = jnp.sum(earlier * hit0, 0, keepdims=True)
    slot1 = jnp.sum(earlier * hit1, 0, keepdims=True)
    place0 = (first ^ e) * capacity + slot0.astype(jnp.int32)
    place1 = (second ^ e) * capacity + slot1.astype(jnp.int32)
    slot_row = lax.broadcasted_iota(jnp.int32, (slots, rows), 0)
    at0, at1 = slot_row == place0, slot_row == place1
    select[...] = (at0.astype(F32) + at1.astype(F32)).astype(BF16)

    values = tokens_ref[...].astype(F32)
    scale = lax.rsqrt(jnp.mean(values * values, -1, keepdims=True) + 1e-06)
    normed[...] = (values * scale * gain_ref[...]).astype(BF16)

    for h in range(2):
        part = normed[:, pl.ds(pl.multiple_of(((t + 2 * h) % 4) * quarter, quarter), quarter)]
        packed = jnp.dot(select[...], part, preferred_element_type=F32).astype(BF16)
        outgoing[h] = packed.reshape(n_ep, capacity, quarter)

    SCOPE("w_barrier", lambda: pl.semaphore_wait(barrier, 2 * n_ep))

    def remote(source, target, send, recv, ep, tp):
        return pltpu.make_async_remote_copy(
            src_ref=source, dst_ref=target, send_sem=send, recv_sem=recv,
            device_id={"ep": ep, "tp": tp}, device_id_type=MESH)

    def landed(ref, sem):
        pltpu.make_async_copy(ref, ref, sem).wait()

    own_half = pl.ds(2 * x, 2)
    for r in range(1, n_ep // 2):
        for h in range(2):
            remote(
                outgoing.at[h, r], arrived.at[r // 2, (t + 2 * h) % 4], send_disp.at[0], recv_disp.at[r // 2],
                toggled(e, r), 2 * x + r % 2).start()
    for far in (outer, 1 - outer):
        for odd in range(2):
            peer = e + flipped(e, 4) + far * flipped(e, 2) + odd * flipped(e, 1)
            remote(
                outgoing.at[0, 4 + 2 * far + odd], arrived.at[2 + far, t], send_disp.at[0], recv_disp.at[2 + far],
                peer, 2 * x + odd).start()
    other = pl.ds(pl.multiple_of((1 - x) * half, half), half)
    shares = [
        remote(down_ref.at[:, other], down_rows.at[x, c, pl.ds(0, width)], send_weight.at[0], recv_weight.at[0], e, across),
        remote(gate_ref, gate_up.at[0, c, pl.ds(0, width)], send_weight.at[1], recv_weight.at[1], e, partner),
        remote(up_ref, gate_up.at[1, c, pl.ds(0, width)], send_weight.at[2], recv_weight.at[2], e, partner),
        remote(down_ref.at[:, columns], down_rows.at[x, c, pl.ds(0, width)], send_weight.at[3], recv_weight.at[3], e, partner),
    ]
    for share in shares:
        share.start()
    far_rows = down_rows.at[1 - x, c, pl.ds(0, width)]
    relay = remote(far_rows, far_rows, send_weight.at[4], recv_weight.at[4], e, partner)

    if fpad > width:
        gate_up[:, :, width:fpad] = jnp.zeros((2, 2, fpad - width, model), BF16)
        down_rows[:, :, width:fpad] = jnp.zeros((2, 2, fpad - width, half), BF16)

    logit0, logit1 = logits_ref[0:1, :], logits_ref[1:2, :]
    top = jnp.maximum(logit0, logit1)
    exp0, exp1 = jnp.exp(logit0 - top), jnp.exp(logit1 - top)
    share = prob_ref[...] / (exp0 + exp1)
    weight = jnp.where(at0, share * exp0, 0.0) + jnp.where(at1, share * exp1, 0.0)
    for part in range(2):
        turned = weight[part * (slots // 2):(part + 1) * (slots // 2)].T
        high = turned.astype(BF16)
        weigh[part, 0] = high
        weigh[part, 1] = (turned - high.astype(F32)).astype(BF16)

    def product(left, right):
        return lax.dot_general(left, right, (((1,), (1,)), ((), ())), preferred_element_type=F32)

    def expand(s):
        acc = jnp.zeros((capacity, 4 * fpad), F32)
        for q in range(4):
            columns = gate_up[:, :, :, q * quarter:(q + 1) * quarter].reshape(4 * fpad, quarter)
            acc = acc + product(arrived[s, q], columns)
        gate, up = acc[:, :2 * fpad], acc[:, 2 * fpad:]
        hidden[s, x] = (gate / (1.0 + jnp.exp(-gate)) * up).astype(BF16)
        remote(hidden.at[s, x], hidden.at[s, x], send_hid.at[0], recv_hid.at[s], e, across).start()

    def contract(s):
        SCOPE(f"w_hid{s if isinstance(s, int) else 'f'}", lambda: landed(hidden.at[s, 1 - x], recv_hid.at[s]))
        acc = jnp.zeros((capacity, half), F32)
        for side in range(2):
            acc = acc + jnp.dot(hidden[s, side], down_rows[side].reshape(2 * fpad, half), preferred_element_type=F32)
        for j in range(2):
            result[s, j] = acc[:, j * quarter:(j + 1) * quarter].astype(BF16)

    def take(s):
        mine = arrived.at[s, own_half]
        SCOPE("w_take", lambda: landed(mine, recv_disp.at[s]))
        remote(mine, mine, send_side.at[0], recv_side.at[s - 2], e, across).start()

    def expand_far(s):
        SCOPE("w_side", lambda: landed(arrived.at[s, pl.ds(2 * (1 - x), 2)], recv_side.at[s - 2]))
        expand(s)

    def contract_far(s):
        contract(s)
        odd = c
        peer = e + flipped(e, 4) + (s - 2) * flipped(e, 2) + odd * flipped(e, 1)
        for j in range(2):
            remote(result.at[s, j], returned.at[2 * s + c], send_home.at[1], recv_home.at[2], peer, 2 * x + j).start()

    @pl.when(c == 0)
    def _():
        own = select[0:capacity]
        for q in range(4):
            block = jnp.dot(own, normed[:, q * quarter:(q + 1) * quarter], preferred_element_type=F32)
            arrived[0, q] = block.astype(BF16)

    def weights_ready():
        for fetch in fetches:
            fetch.wait()
        for kind in range(2):
            landed(gate_up.at[kind, 1 - c, pl.ds(0, width)], recv_weight.at[1 + kind])

    SCOPE("w_weights", weights_ready)

    @pl.when(c == 1)
    def _():
        SCOPE("w_near0", lambda: landed(arrived.at[0], recv_disp.at[0]))

    sa, sb = 3 - outer, 2 + outer
    SCOPE("expand0", lambda: expand(0))
    SCOPE("take_a", lambda: take(sa))
    SCOPE("w_near1", lambda: landed(arrived.at[1], recv_disp.at[1]))
    SCOPE("expand1", lambda: expand(1))

    def relay_down():
        landed(far_rows, recv_weight.at[0])
        relay.start()

    SCOPE("relay_down", relay_down)
    SCOPE("expand_a", lambda: expand_far(sa))
    SCOPE("take_b", lambda: take(sb))

    def down_ready():
        landed(down_rows.at[x, 1 - c, pl.ds(0, width)], recv_weight.at[3])
        landed(down_rows.at[1 - x, 1 - c, pl.ds(0, width)], recv_weight.at[4])

    SCOPE("w_down", down_ready)

    def near_home(s):
        contract(s)
        peer = e + (s * flipped(e, 2) if s else 0) + c * flipped(e, 1)
        if s:
            for j in range(2):
                remote(result.at[s, j], returned.at[2 * s + c], send_home.at[0], recv_home.at[1], peer, 2 * x + j).start()
            return

        @pl.when(c == 0)
        def _():
            returned[0] = result[0, 0]
            remote(result.at[0, 1], returned.at[0], send_home.at[2], recv_home.at[0], e, partner).start()

        @pl.when(c == 1)
        def _():
            for j in range(2):
                remote(result.at[0, j], returned.at[1], send_home.at[2], recv_home.at[1], peer, 2 * x + j).start()

    SCOPE("contract0", lambda: near_home(0))
    SCOPE("contract1", lambda: near_home(1))
    SCOPE("contract_a", lambda: contract_far(sa))
    SCOPE("expand_b", lambda: expand_far(sb))
    SCOPE("contract_b", lambda: contract_far(sb))

    def merge(part):
        back = returned[part * (n_ep // 2):(part + 1) * (n_ep // 2)].reshape(slots // 2, quarter)
        return (jnp.dot(weigh[part, 0], back, preferred_element_type=F32)
                + jnp.dot(weigh[part, 1], back, preferred_element_type=F32))

    @pl.when(c == 1)
    def _():
        SCOPE("w_back0", lambda: landed(returned.at[0], recv_home.at[0]))

    SCOPE("w_back1", lambda: landed(returned.at[pl.ds(1, n_ep // 2 - 1)], recv_home.at[1]))
    total = merge(0)
    SCOPE("w_back2", lambda: landed(returned.at[pl.ds(n_ep // 2, n_ep // 2)], recv_home.at[2]))
    out_ref[...] = (total + merge(1)).astype(BF16)

    def finish():
        landed(outgoing.at[:, pl.ds(0, (3 * n_ep // 2 - 2) // 2)], send_disp.at[0])
        landed(arrived.at[pl.ds(0, 2), own_half], send_side.at[0])
        landed(hidden.at[:, x], send_hid.at[0])
        landed(result.at[1], send_home.at[0])
        landed(result.at[pl.ds(2, 2)], send_home.at[1])

        @pl.when(c == 0)
        def _():
            landed(result.at[0, 1], send_home.at[2])

        @pl.when(c == 1)
        def _():
            landed(result.at[0], send_home.at[2])

        for share in shares:
            share.wait_send()
        relay.wait_send()

    SCOPE("w_sends", finish)


def fused_body(tokens, norm_gain, routes, group_prob, expert_logits, gate_weight, up_weight, down_matrix):
    n_ep = lax.axis_size("ep")
    rows, model = tokens.shape
    capacity = 3 * routes.shape[1] * rows // (2 * n_ep)
    width = gate_weight.shape[2]
    fpad = round_up(width, 128)
    half, quarter = model // 2, model // 4
    sem = pltpu.SemaphoreType.DMA
    vmem = pl.BlockSpec(memory_space=pltpu.VMEM)
    operands = (
        tokens, norm_gain.reshape(1, model), routes.T, group_prob.reshape(1, rows), expert_logits.T,
        gate_weight.reshape(model, width).T, up_weight.reshape(model, width).T, down_matrix.reshape(width, model),
    )
    return pl.pallas_call(
        functools.partial(expert_kernel, n_ep, capacity, width),
        out_shape=jax.ShapeDtypeStruct((rows, quarter), BF16),
        in_specs=[pl.BlockSpec(memory_space=pl.ANY)] * 8,
        out_specs=vmem,
        scratch_shapes=[
            pltpu.VMEM((rows, model), BF16),
            pltpu.VMEM((1, model), F32),
            pltpu.VMEM((2, rows), jnp.int32),
            pltpu.VMEM((1, rows), F32),
            pltpu.VMEM((2, rows), F32),
            pltpu.VMEM((rows, model), BF16),
            pltpu.VMEM((n_ep * capacity, rows), BF16),
            pltpu.VMEM((2, 2, rows, n_ep * capacity // 2), BF16),
            pltpu.VMEM((2, n_ep, capacity, quarter), BF16),
            pltpu.VMEM((n_ep // 2, 4, capacity, quarter), BF16),
            pltpu.VMEM((2, 2, fpad, model), BF16),
            pltpu.VMEM((2, 2, fpad, half), BF16),
            pltpu.VMEM((n_ep // 2, 2, capacity, 2 * fpad), BF16),
            pltpu.VMEM((n_ep // 2, 2, capacity, quarter), BF16),
            pltpu.VMEM((n_ep, capacity, quarter), BF16),
            sem((8,)),
            sem((1,)), sem((n_ep // 2,)),
            sem((1,)), sem((2,)),
            sem((1,)), sem((n_ep // 2,)),
            sem((3,)), sem((3,)),
            sem((5,)), sem((5,)),
        ],
        compiler_params=pltpu.CompilerParams(
            collective_id=0, has_side_effects=True, vmem_limit_bytes=32 * 1024 * 1024),
    )(*[pltpu.with_memory_space_constraint(operand, pltpu.HBM) for operand in operands])


def fits_kernel(n_ep, n_tp, rows, experts, top, model):
    capacity = 3 * top * rows // (2 * experts)
    return (
        experts == n_ep and top == 2 and n_ep == 8 and n_tp == 4
        and capacity % 16 == 0 and rows % 128 == 0 and model % 512 == 0
    )


def solution(mesh):
    n_ep, n_tp = mesh.shape["ep"], mesh.shape["tp"]

    def chosen(*arrays):
        rows, model = arrays[0].shape
        fits = fits_kernel(n_ep, n_tp, rows, arrays[5].shape[0] * n_ep, arrays[2].shape[1], model)
        return (fused_body if fits else body)(*arrays)

    return jax.shard_map(
        chosen,
        mesh=mesh,
        in_specs=(
            P("ep", None),
            P(),
            P("ep", None),
            P("ep"),
            P("ep", None),
            P("ep", None, "tp"),
            P("ep", None, "tp"),
            P("ep", "tp", None),
        ),
        out_specs=P("ep", "tp"),
        check_vma=False,
    )
```

time: 38 us -> 31.8 us (0.84)
  Pallas kernels: 37.2 us -> 30.7 us
    pallas_call x1, Pallas kernels: 37.2 us -> 30.7 us  [fused_body(): pl.pallas_call(functools.partial(expert_kernel, n_ep, capacity, width), o...]
where the time goes in v2:
time: 31.8 us; the launch traced here: 31.4 us
  Pallas kernels  30.7 us (97%)
  local copies, waits for them, and re-layouts  0.66 us (2%)
    pallas_call x1, Pallas kernels, fused_body(): pl.pallas_call(functools.partial(expert_kernel, n_ep, capacity, width), o...  30.7 us
    unnamed x1, local copies, waits for them, and re-layouts  0.66 us

profile of v2, /device:TPU:0, one launch (start us, length us, event | category | flops | bytes accessed | tf_op | source)
XLA Modules:
  0.0 31.4 jit_solution(5410775315543991189)
XLA Ops:
  0.0 30.7 %shard_map.82 = bf16[128,512]{1,0:T(8,128)(2,1)S(1)} custom-call(bf16[128,2048]{1,0:T(8,128)(2,1)} %tokens_hbm.1, f32[1,2048]{1,0:T(1,128)} %bitcast.14, s32[2,128]{1,0:T(2,128)} %bitcast.15, f32[1,128]{1,0:T(1,128)} %bitcast.17, f32[2,128]{1,0:T(2,128)} %bitcast.16, bf16[96,2048]{1,0:T(8,128)(2,1)} %bitcast.11, bf16[96,2048]{1,0:T(8,128)(2,1)} %bitcast.12, ...), custom_call_target="tpu_custom_call" | custom-call | tf_op jit(solution)/shard_map/pallas_call | solution.py:367
  30.7 0.7 %copy.10 = bf16[128,512]{1,0:T(8,128)(2,1)} copy(bf16[128,512]{1,0:T(8,128)(2,1)S(1)} %shard_map.82) | data formatting | bytes 262144

commit v3 on v2

--- a/solution.py
+++ b/solution.py
@@ -79,10 +79,6 @@
     return -(-value // step) * step
 
 
-def SCOPE(name, run):
-    run()
-
-
 def flipped(index, bit):
     return bit * (1 - 2 * ((index // bit) % 2))
 
@@ -100,8 +96,8 @@
     n_ep, capacity, width,
     tokens_hbm, gain_hbm, routes_hbm, prob_hbm, logits_hbm, gate_ref, up_ref, down_ref,
     out_ref,
-    tokens_ref, gain_ref, routes_ref, prob_ref, logits_ref, normed, select, weigh, outgoing, arrived, gate_up, down_rows,
-    hidden, result, returned,
+    tokens_ref, gain_ref, routes_ref, prob_ref, logits_ref, normed, select, weigh, leaving, outgoing, arrived, gate_up,
+    down_rows, down_other, hidden, result, returned,
     load_sem, send_disp, recv_disp, send_side, recv_side, send_hid, recv_hid, send_home, recv_home, send_weight, recv_weight,
 ):
     loads = [
@@ -116,6 +112,7 @@
     rows, model = tokens_ref.shape
     half, quarter = model // 2, model // 4
     fpad = gate_up.shape[2]
+    near = n_ep // 2
     slots = n_ep * capacity
     e = lax.axis_index("ep")
     t = lax.axis_index("tp")
@@ -124,22 +121,26 @@
     outer = 1 - ((e // 2) % 2 + (e // 4) % 2) % 2
 
     barrier = pltpu.get_barrier_semaphore()
-    for r in range(n_ep):
+    for r in reversed(range(n_ep)):
         for mate in (t, partner):
             if r or mate is partner:
                 pl.semaphore_signal(
                     barrier, inc=1, device_id={"ep": toggled(e, r), "tp": mate}, device_id_type=MESH)
     pl.semaphore_signal(barrier, inc=1, device_id={"ep": e, "tp": across}, device_id_type=MESH)
 
-    columns = pl.ds(pl.multiple_of(x * half, half), half)
+    def columns(side):
+        return pl.ds(pl.multiple_of(side * half, half), half)
+
     fetches = [
-        pltpu.make_async_copy(gate_ref, gate_up.at[0, c, pl.ds(0, width)], load_sem.at[5]),
-        pltpu.make_async_copy(up_ref, gate_up.at[1, c, pl.ds(0, width)], load_sem.at[6]),
-        pltpu.make_async_copy(down_ref.at[:, columns], down_rows.at[x, c, pl.ds(0, width)], load_sem.at[7]),
+        pltpu.make_async_copy(down_ref.at[:, columns(1 - x)], down_other, load_sem.at[5]),
+        pltpu.make_async_copy(gate_ref, gate_up.at[0, c, pl.ds(0, width)], load_sem.at[6]),
+        pltpu.make_async_copy(up_ref, gate_up.at[1, c, pl.ds(0, width)], load_sem.at[7]),
+        pltpu.make_async_copy(down_ref.at[:, columns(x)], down_rows.at[x, c, pl.ds(0, width)], load_sem.at[8]),
     ]
     for fetch in fetches:
         fetch.start()
-    SCOPE("w_loads", lambda: [load.wait() for load in loads])
+    for load in loads:
+        load.wait()
 
     first, second = routes_ref[0:1, :], routes_ref[1:2, :]
     lanes = round_up(n_ep, 16)
@@ -162,12 +163,23 @@
     scale = lax.rsqrt(jnp.mean(values * values, -1, keepdims=True) + 1e-06)
     normed[...] = (values * scale * gain_ref[...]).astype(BF16)
 
-    for h in range(2):
-        part = normed[:, pl.ds(pl.multiple_of(((t + 2 * h) % 4) * quarter, quarter), quarter)]
-        packed = jnp.dot(select[...], part, preferred_element_type=F32).astype(BF16)
-        outgoing[h] = packed.reshape(n_ep, capacity, quarter)
-
-    SCOPE("w_barrier", lambda: pl.semaphore_wait(barrier, 2 * n_ep))
+    def packed(begin, end, lanes):
+        return jnp.dot(
+            select[begin * capacity:end * capacity], normed[:, lanes], preferred_element_type=F32
+        ).astype(BF16).reshape(end - begin, capacity, half)
+
+    @pl.when(c == 1)
+    def _():
+        leaving[...] = packed(near, n_ep, columns(x))
+
+    @pl.when(c == 0)
+    def _():
+        for side in range(2):
+            both = packed(0, 2, slice(side * half, (side + 1) * half))
+            arrived[0, side] = both[0]
+            outgoing[0, side] = both[1]
+
+    pl.semaphore_wait(barrier, 2 * n_ep)
 
     def remote(source, target, send, recv, ep, tp):
         return pltpu.make_async_remote_copy(
@@ -177,28 +189,38 @@
     def landed(ref, sem):
         pltpu.make_async_copy(ref, ref, sem).wait()
 
-    own_half = pl.ds(2 * x, 2)
-    for r in range(1, n_ep // 2):
-        for h in range(2):
-            remote(
-                outgoing.at[h, r], arrived.at[r // 2, (t + 2 * h) % 4], send_disp.at[0], recv_disp.at[r // 2],
-                toggled(e, r), 2 * x + r % 2).start()
-    for far in (outer, 1 - outer):
-        for odd in range(2):
-            peer = e + flipped(e, 4) + far * flipped(e, 2) + odd * flipped(e, 1)
-            remote(
-                outgoing.at[0, 4 + 2 * far + odd], arrived.at[2 + far, t], send_disp.at[0], recv_disp.at[2 + far],
-                peer, 2 * x + odd).start()
-    other = pl.ds(pl.multiple_of((1 - x) * half, half), half)
+    def far_peer(step, odd):
+        return e + flipped(e, 4) + step * flipped(e, 2) + odd * flipped(e, 1)
+
+    @pl.when(c == 1)
+    def _():
+        for step in (outer, 1 - outer):
+            for odd in range(2):
+                s = 2 * step + odd
+                remote(
+                    leaving.at[s], arrived.at[s, x], send_disp.at[0], recv_disp.at[s], far_peer(step, odd), t).start()
+        for side in range(2):
+            outgoing[0:2, side] = packed(2, 4, slice(side * half, (side + 1) * half))
+        for s in (3, 2):
+            remote(outgoing.at[s - 2], arrived.at[s], send_disp.at[1], recv_disp.at[s], toggled(e, s), partner).start()
+
+    @pl.when(c == 0)
+    def _():
+        remote(outgoing.at[0], arrived.at[1], send_disp.at[0], recv_disp.at[1], toggled(e, 1), t).start()
+
+    def owned(ref, side, core):
+        return ref.at[side, core, pl.ds(0, width)]
+
     shares = [
-        remote(down_ref.at[:, other], down_rows.at[x, c, pl.ds(0, width)], send_weight.at[0], recv_weight.at[0], e, across),
-        remote(gate_ref, gate_up.at[0, c, pl.ds(0, width)], send_weight.at[1], recv_weight.at[1], e, partner),
-        remote(up_ref, gate_up.at[1, c, pl.ds(0, width)], send_weight.at[2], recv_weight.at[2], e, partner),
-        remote(down_ref.at[:, columns], down_rows.at[x, c, pl.ds(0, width)], send_weight.at[3], recv_weight.at[3], e, partner),
+        remote(down_other, owned(down_rows, x, c), send_weight.at[0], recv_weight.at[0], e, across),
+        remote(owned(gate_up, 0, c), owned(gate_up, 0, c), send_weight.at[1], recv_weight.at[1], e, partner),
+        remote(owned(gate_up, 1, c), owned(gate_up, 1, c), send_weight.at[2], recv_weight.at[2], e, partner),
+        remote(owned(down_rows, x, c), owned(down_rows, x, c), send_weight.at[3], recv_weight.at[3], e, partner),
     ]
-    for share in shares:
+    for fetch, share in zip(fetches, shares):
+        fetch.wait()
         share.start()
-    far_rows = down_rows.at[1 - x, c, pl.ds(0, width)]
+    far_rows = owned(down_rows, 1 - x, c)
     relay = remote(far_rows, far_rows, send_weight.at[4], recv_weight.at[4], e, partner)
 
     if fpad > width:
@@ -219,136 +241,134 @@
     def product(left, right):
         return lax.dot_general(left, right, (((1,), (1,)), ((), ())), preferred_element_type=F32)
 
+    def take(s):
+        mine = arrived.at[s, x]
+        landed(mine, recv_disp.at[s])
+        remote(mine, mine, send_side.at[0], recv_side.at[s], e, across).start()
+
     def expand(s):
         acc = jnp.zeros((capacity, 4 * fpad), F32)
         for q in range(4):
-            columns = gate_up[:, :, :, q * quarter:(q + 1) * quarter].reshape(4 * fpad, quarter)
-            acc = acc + product(arrived[s, q], columns)
+            part = arrived[s, q // 2, :, (q % 2) * quarter:(q % 2 + 1) * quarter]
+            acc = acc + product(part, gate_up[:, :, :, q * quarter:(q + 1) * quarter].reshape(4 * fpad, quarter))
         gate, up = acc[:, :2 * fpad], acc[:, 2 * fpad:]
         hidden[s, x] = (gate / (1.0 + jnp.exp(-gate)) * up).astype(BF16)
         remote(hidden.at[s, x], hidden.at[s, x], send_hid.at[0], recv_hid.at[s], e, across).start()
 
     def contract(s):
-        SCOPE(f"w_hid{s if isinstance(s, int) else 'f'}", lambda: landed(hidden.at[s, 1 - x], recv_hid.at[s]))
+        landed(hidden.at[s, 1 - x], recv_hid.at[s])
         acc = jnp.zeros((capacity, half), F32)
         for side in range(2):
             acc = acc + jnp.dot(hidden[s, side], down_rows[side].reshape(2 * fpad, half), preferred_element_type=F32)
         for j in range(2):
             result[s, j] = acc[:, j * quarter:(j + 1) * quarter].astype(BF16)
 
-    def take(s):
-        mine = arrived.at[s, own_half]
-        SCOPE("w_take", lambda: landed(mine, recv_disp.at[s]))
-        remote(mine, mine, send_side.at[0], recv_side.at[s - 2], e, across).start()
-
-    def expand_far(s):
-        SCOPE("w_side", lambda: landed(arrived.at[s, pl.ds(2 * (1 - x), 2)], recv_side.at[s - 2]))
-        expand(s)
-
-    def contract_far(s):
-        contract(s)
-        odd = c
-        peer = e + flipped(e, 4) + (s - 2) * flipped(e, 2) + odd * flipped(e, 1)
+    def home(s, r, peer, group):
         for j in range(2):
-            remote(result.at[s, j], returned.at[2 * s + c], send_home.at[1], recv_home.at[2], peer, 2 * x + j).start()
-
-    @pl.when(c == 0)
-    def _():
-        own = select[0:capacity]
-        for q in range(4):
-            block = jnp.dot(own, normed[:, q * quarter:(q + 1) * quarter], preferred_element_type=F32)
-            arrived[0, q] = block.astype(BF16)
+            remote(result.at[s, j], returned.at[r], send_home.at[0], recv_home.at[group], peer, 2 * x + j).start()
 
     def weights_ready():
-        for fetch in fetches:
-            fetch.wait()
         for kind in range(2):
-            landed(gate_up.at[kind, 1 - c, pl.ds(0, width)], recv_weight.at[1 + kind])
-
-    SCOPE("w_weights", weights_ready)
-
-    @pl.when(c == 1)
-    def _():
-        SCOPE("w_near0", lambda: landed(arrived.at[0], recv_disp.at[0]))
-
-    sa, sb = 3 - outer, 2 + outer
-    SCOPE("expand0", lambda: expand(0))
-    SCOPE("take_a", lambda: take(sa))
-    SCOPE("w_near1", lambda: landed(arrived.at[1], recv_disp.at[1]))
-    SCOPE("expand1", lambda: expand(1))
+            landed(owned(gate_up, kind, 1 - c), recv_weight.at[1 + kind])
 
     def relay_down():
         landed(far_rows, recv_weight.at[0])
         relay.start()
 
-    SCOPE("relay_down", relay_down)
-    SCOPE("expand_a", lambda: expand_far(sa))
-    SCOPE("take_b", lambda: take(sb))
-
     def down_ready():
-        landed(down_rows.at[x, 1 - c, pl.ds(0, width)], recv_weight.at[3])
-        landed(down_rows.at[1 - x, 1 - c, pl.ds(0, width)], recv_weight.at[4])
-
-    SCOPE("w_down", down_ready)
-
-    def near_home(s):
-        contract(s)
-        peer = e + (s * flipped(e, 2) if s else 0) + c * flipped(e, 1)
-        if s:
-            for j in range(2):
-                remote(result.at[s, j], returned.at[2 * s + c], send_home.at[0], recv_home.at[1], peer, 2 * x + j).start()
-            return
-
-        @pl.when(c == 0)
-        def _():
-            returned[0] = result[0, 0]
-            remote(result.at[0, 1], returned.at[0], send_home.at[2], recv_home.at[0], e, partner).start()
-
-        @pl.when(c == 1)
-        def _():
-            for j in range(2):
-                remote(result.at[0, j], returned.at[1], send_home.at[2], recv_home.at[1], peer, 2 * x + j).start()
-
-    SCOPE("contract0", lambda: near_home(0))
-    SCOPE("contract1", lambda: near_home(1))
-    SCOPE("contract_a", lambda: contract_far(sa))
-    SCOPE("expand_b", lambda: expand_far(sb))
-    SCOPE("contract_b", lambda: contract_far(sb))
+        landed(owned(down_rows, x, 1 - c), recv_weight.at[3])
+        landed(owned(down_rows, 1 - x, 1 - c), recv_weight.at[4])
 
     def merge(part):
-        back = returned[part * (n_ep // 2):(part + 1) * (n_ep // 2)].reshape(slots // 2, quarter)
+        back = returned[part * near:(part + 1) * near].reshape(slots // 2, quarter)
         return (jnp.dot(weigh[part, 0], back, preferred_element_type=F32)
                 + jnp.dot(weigh[part, 1], back, preferred_element_type=F32))
 
     @pl.when(c == 1)
     def _():
-        SCOPE("w_back0", lambda: landed(returned.at[0], recv_home.at[0]))
-
-    SCOPE("w_back1", lambda: landed(returned.at[pl.ds(1, n_ep // 2 - 1)], recv_home.at[1]))
+        order = [(2 * step + odd, step, odd) for step in (outer, 1 - outer) for odd in range(2)]
+
+        def far_take(i):
+            take(order[i][0])
+
+        def far_expand(i):
+            s = order[i][0]
+            landed(arrived.at[s, 1 - x], recv_side.at[s])
+            expand(s)
+
+        def far_contract(i):
+            s, step, odd = order[i]
+            contract(s)
+            home(s, near + s, far_peer(step, odd), 2)
+
+        far_take(0)
+        far_take(1)
+        weights_ready()
+        relay_down()
+        far_expand(0)
+        far_take(2)
+        far_expand(1)
+        far_take(3)
+        down_ready()
+        far_contract(0)
+        far_contract(1)
+        far_expand(2)
+        far_expand(3)
+        far_contract(2)
+        far_contract(3)
+        landed(returned.at[0], recv_home.at[0])
+
+    @pl.when(c == 0)
+    def _():
+        def near_expand(s):
+            if s:
+                landed(arrived.at[s], recv_disp.at[s])
+            expand(s)
+
+        def near_contract(s):
+            contract(s)
+            if s:
+                home(s, s, toggled(e, s), 1)
+            else:
+                returned[0] = result[0, 0]
+                remote(result.at[0, 1], returned.at[0], send_home.at[0], recv_home.at[0], e, partner).start()
+
+        weights_ready()
+        near_expand(0)
+        near_expand(1)
+        relay_down()
+        down_ready()
+        near_contract(0)
+        near_contract(1)
+        near_expand(3)
+        near_expand(2)
+        near_contract(3)
+        near_contract(2)
+
+    landed(returned.at[pl.ds(1, near - 1)], recv_home.at[1])
     total = merge(0)
-    SCOPE("w_back2", lambda: landed(returned.at[pl.ds(n_ep // 2, n_ep // 2)], recv_home.at[2]))
+    landed(returned.at[pl.ds(near, near)], recv_home.at[2])
     out_ref[...] = (total + merge(1)).astype(BF16)
 
     def finish():
-        landed(outgoing.at[:, pl.ds(0, (3 * n_ep // 2 - 2) // 2)], send_disp.at[0])
-        landed(arrived.at[pl.ds(0, 2), own_half], send_side.at[0])
         landed(hidden.at[:, x], send_hid.at[0])
-        landed(result.at[1], send_home.at[0])
-        landed(result.at[pl.ds(2, 2)], send_home.at[1])
-
-        @pl.when(c == 0)
-        def _():
-            landed(result.at[0, 1], send_home.at[2])
-
-        @pl.when(c == 1)
-        def _():
-            landed(result.at[0], send_home.at[2])
-
         for share in shares:
             share.wait_send()
         relay.wait_send()
 
-    SCOPE("w_sends", finish)
+        @pl.when(c == 1)
+        def _():
+            landed(leaving, send_disp.at[0])
+            landed(outgoing, send_disp.at[1])
+            landed(arrived.at[:, x], send_side.at[0])
+            landed(result, send_home.at[0])
+
+        @pl.when(c == 0)
+        def _():
+            landed(outgoing.at[0], send_disp.at[0])
+            landed(returned.at[pl.ds(0, 2 * near - 1)], send_home.at[0])
+
+    finish()
 
 
 def fused_body(tokens, norm_gain, routes, group_prob, expert_logits, gate_weight, up_weight, down_matrix):
@@ -378,18 +398,20 @@
             pltpu.VMEM((rows, model), BF16),
             pltpu.VMEM((n_ep * capacity, rows), BF16),
             pltpu.VMEM((2, 2, rows, n_ep * capacity // 2), BF16),
-            pltpu.VMEM((2, n_ep, capacity, quarter), BF16),
-            pltpu.VMEM((n_ep // 2, 4, capacity, quarter), BF16),
+            pltpu.VMEM((n_ep // 2, capacity, half), BF16),
+            pltpu.VMEM((2, 2, capacity, half), BF16),
+            pltpu.VMEM((n_ep // 2, 2, capacity, half), BF16),
             pltpu.VMEM((2, 2, fpad, model), BF16),
             pltpu.VMEM((2, 2, fpad, half), BF16),
+            pltpu.VMEM((width, half), BF16),
             pltpu.VMEM((n_ep // 2, 2, capacity, 2 * fpad), BF16),
             pltpu.VMEM((n_ep // 2, 2, capacity, quarter), BF16),
             pltpu.VMEM((n_ep, capacity, quarter), BF16),
-            sem((8,)),
+            sem((9,)),
+            sem((2,)), sem((n_ep // 2,)),
             sem((1,)), sem((n_ep // 2,)),
-            sem((1,)), sem((2,)),
             sem((1,)), sem((n_ep // 2,)),
-            sem((3,)), sem((3,)),
+            sem((1,)), sem((3,)),
             sem((5,)), sem((5,)),
         ],
         compiler_params=pltpu.CompilerParams(

time: 31.8 us -> 28.4 us (0.89)
  Pallas kernels: 30.7 us -> 27.2 us
    pallas_call x1, Pallas kernels: 30.7 us -> 27.2 us  [fused_body(): pl.pallas_call(functools.partial(expert_kernel, n_ep, capacity, width), o...]
where the time goes in v3:
time: 28.4 us; the launch traced here: 27.9 us
  Pallas kernels  27.2 us (96%)
  local copies, waits for them, and re-layouts  0.66 us (2%)
    pallas_call x1, Pallas kernels, fused_body(): pl.pallas_call(functools.partial(expert_kernel, n_ep, capacity, width), o...  27.2 us
    unnamed x1, local copies, waits for them, and re-layouts  0.66 us

profile of v3, /device:TPU:0, one launch (start us, length us, event | category | flops | bytes accessed | tf_op | source)
XLA Modules:
  0.0 27.9 jit_solution(7236674372391093409)
XLA Ops:
  0.0 27.2 %shard_map.82 = bf16[128,512]{1,0:T(8,128)(2,1)S(1)} custom-call(bf16[128,2048]{1,0:T(8,128)(2,1)} %tokens_hbm.1, f32[1,2048]{1,0:T(1,128)} %bitcast.14, s32[2,128]{1,0:T(2,128)} %bitcast.15, f32[1,128]{1,0:T(1,128)} %bitcast.17, f32[2,128]{1,0:T(2,128)} %bitcast.16, bf16[96,2048]{1,0:T(8,128)(2,1)} %bitcast.11, bf16[96,2048]{1,0:T(8,128)(2,1)} %bitcast.12, ...), custom_call_target="tpu_custom_call" | custom-call | tf_op jit(solution)/shard_map/pallas_call | solution.py:387
  27.2 0.7 %copy.10 = bf16[128,512]{1,0:T(8,128)(2,1)} copy(bf16[128,512]{1,0:T(8,128)(2,1)S(1)} %shard_map.82) | data formatting | bytes 262144

commit v4 on v3

--- a/solution.py
+++ b/solution.py
@@ -96,7 +96,7 @@
     n_ep, capacity, width,
     tokens_hbm, gain_hbm, routes_hbm, prob_hbm, logits_hbm, gate_ref, up_ref, down_ref,
     out_ref,
-    tokens_ref, gain_ref, routes_ref, prob_ref, logits_ref, normed, select, weigh, leaving, outgoing, arrived, gate_up,
+    tokens_ref, gain_ref, routes_ref, prob_ref, logits_ref, normed, select, weigh, leaving, spare, outgoing, arrived, gate_up,
     down_rows, down_other, hidden, result, returned,
     load_sem, send_disp, recv_disp, send_side, recv_side, send_hid, recv_hid, send_home, recv_home, send_weight, recv_weight,
 ):
@@ -111,7 +111,6 @@
         load.start()
     rows, model = tokens_ref.shape
     half, quarter = model // 2, model // 4
-    fpad = gate_up.shape[2]
     near = n_ep // 2
     slots = n_ep * capacity
     e = lax.axis_index("ep")
@@ -120,6 +119,8 @@
     partner, across = t + 1 - 2 * c, (t + 2) % 4
     outer = 1 - ((e // 2) % 2 + (e // 4) % 2) % 2
 
+    hi, lo = e // 4, (e // 2) % 2
+
     barrier = pltpu.get_barrier_semaphore()
     for r in reversed(range(n_ep)):
         for mate in (t, partner):
@@ -131,11 +132,14 @@
     def columns(side):
         return pl.ds(pl.multiple_of(side * half, half), half)
 
+    def owned(ref, side, core):
+        return ref.at[side, pl.ds(pl.multiple_of(core * width, width), width)]
+
     fetches = [
         pltpu.make_async_copy(down_ref.at[:, columns(1 - x)], down_other, load_sem.at[5]),
-        pltpu.make_async_copy(gate_ref, gate_up.at[0, c, pl.ds(0, width)], load_sem.at[6]),
-        pltpu.make_async_copy(up_ref, gate_up.at[1, c, pl.ds(0, width)], load_sem.at[7]),
-        pltpu.make_async_copy(down_ref.at[:, columns(x)], down_rows.at[x, c, pl.ds(0, width)], load_sem.at[8]),
+        pltpu.make_async_copy(gate_ref, owned(gate_up, 0, c), load_sem.at[6]),
+        pltpu.make_async_copy(up_ref, owned(gate_up, 1, c), load_sem.at[7]),
+        pltpu.make_async_copy(down_ref.at[:, columns(x)], owned(down_rows, x, c), load_sem.at[8]),
     ]
     for fetch in fetches:
         fetch.start()
@@ -192,15 +196,33 @@
     def far_peer(step, odd):
         return e + flipped(e, 4) + step * flipped(e, 2) + odd * flipped(e, 1)
 
-    @pl.when(c == 1)
-    def _():
-        for step in (outer, 1 - outer):
-            for odd in range(2):
-                s = 2 * step + odd
-                remote(
-                    leaving.at[s], arrived.at[s, x], send_disp.at[0], recv_disp.at[s], far_peer(step, odd), t).start()
+    def send_far(step):
+        for odd in range(2):
+            s = 2 * step + odd
+            remote(leaving.at[s], arrived.at[s, x], send_disp.at[0], recv_disp.at[s], far_peer(step, odd), t).start()
+
+    def pack_near():
         for side in range(2):
             outgoing[0:2, side] = packed(2, 4, slice(side * half, (side + 1) * half))
+
+    first_step = outer
+
+    @pl.when(c == 1)
+    def _():
+        send_far(first_step)
+        send_far(1 - first_step)
+
+        @pl.when(outer == 0)
+        def _():
+            spare[...] = packed(n_ep - 1, n_ep, columns(1 - x))[0]
+            remote(spare, arrived.at[3, 1 - x], send_disp.at[2], recv_side.at[3], far_peer(1, 1), t).start()
+
+    @pl.when(c == 1)
+    def _():
+        pack_near()
+
+    @pl.when(c == 1)
+    def _():
         for s in (3, 2):
             remote(outgoing.at[s - 2], arrived.at[s], send_disp.at[1], recv_disp.at[s], toggled(e, s), partner).start()
 
@@ -208,24 +230,20 @@
     def _():
         remote(outgoing.at[0], arrived.at[1], send_disp.at[0], recv_disp.at[1], toggled(e, 1), t).start()
 
-    def owned(ref, side, core):
-        return ref.at[side, core, pl.ds(0, width)]
+    shed = remote(down_other, owned(down_rows, x, c), send_weight.at[0], recv_weight.at[0], e, across)
+    fetches[0].wait()
+    shed.start()
 
     shares = [
-        remote(down_other, owned(down_rows, x, c), send_weight.at[0], recv_weight.at[0], e, across),
         remote(owned(gate_up, 0, c), owned(gate_up, 0, c), send_weight.at[1], recv_weight.at[1], e, partner),
         remote(owned(gate_up, 1, c), owned(gate_up, 1, c), send_weight.at[2], recv_weight.at[2], e, partner),
         remote(owned(down_rows, x, c), owned(down_rows, x, c), send_weight.at[3], recv_weight.at[3], e, partner),
     ]
-    for fetch, share in zip(fetches, shares):
+    for fetch, share in zip(fetches[1:], shares):
         fetch.wait()
         share.start()
     far_rows = owned(down_rows, 1 - x, c)
     relay = remote(far_rows, far_rows, send_weight.at[4], recv_weight.at[4], e, partner)
-
-    if fpad > width:
-        gate_up[:, :, width:fpad] = jnp.zeros((2, 2, fpad - width, model), BF16)
-        down_rows[:, :, width:fpad] = jnp.zeros((2, 2, fpad - width, half), BF16)
 
     logit0, logit1 = logits_ref[0:1, :], logits_ref[1:2, :]
     top = jnp.maximum(logit0, logit1)
@@ -241,25 +259,36 @@
     def product(left, right):
         return lax.dot_general(left, right, (((1,), (1,)), ((), ())), preferred_element_type=F32)
 
-    def take(s):
+    def take(s, on=True):
         mine = arrived.at[s, x]
         landed(mine, recv_disp.at[s])
-        remote(mine, mine, send_side.at[0], recv_side.at[s], e, across).start()
-
-    def expand(s):
-        acc = jnp.zeros((capacity, 4 * fpad), F32)
-        for q in range(4):
-            part = arrived[s, q // 2, :, (q % 2) * quarter:(q % 2 + 1) * quarter]
-            acc = acc + product(part, gate_up[:, :, :, q * quarter:(q + 1) * quarter].reshape(4 * fpad, quarter))
-        gate, up = acc[:, :2 * fpad], acc[:, 2 * fpad:]
+
+        def pass_on():
+            remote(mine, mine, send_side.at[0], recv_side.at[s], e, across).start()
+
+        if on is True:
+            pass_on()
+        else:
+            pl.when(on)(pass_on)
+
+    def expand(s, begin=0, wait=None):
+        gate = jnp.zeros((capacity, 2 * width), F32)
+        up = jnp.zeros((capacity, 2 * width), F32)
+        for side in (begin, 1 - begin):
+            if wait is not None and side is not begin:
+                wait()
+            for q in range(2):
+                part = arrived[s, side, :, q * quarter:(q + 1) * quarter]
+                lanes = pl.ds(pl.multiple_of(side * half + q * quarter, quarter), quarter)
+                gate = gate + product(part, gate_up[0, :, lanes])
+                up = up + product(part, gate_up[1, :, lanes])
         hidden[s, x] = (gate / (1.0 + jnp.exp(-gate)) * up).astype(BF16)
         remote(hidden.at[s, x], hidden.at[s, x], send_hid.at[0], recv_hid.at[s], e, across).start()
 
     def contract(s):
+        acc = jnp.dot(hidden[s, x], down_rows[x], preferred_element_type=F32)
         landed(hidden.at[s, 1 - x], recv_hid.at[s])
-        acc = jnp.zeros((capacity, half), F32)
-        for side in range(2):
-            acc = acc + jnp.dot(hidden[s, side], down_rows[side].reshape(2 * fpad, half), preferred_element_type=F32)
+        acc = acc + jnp.dot(hidden[s, 1 - x], down_rows[1 - x], preferred_element_type=F32)
         for j in range(2):
             result[s, j] = acc[:, j * quarter:(j + 1) * quarter].astype(BF16)
 
@@ -286,15 +315,17 @@
 
     @pl.when(c == 1)
     def _():
-        order = [(2 * step + odd, step, odd) for step in (outer, 1 - outer) for odd in range(2)]
+        order = [
+            (2 * step + odd, step, odd)
+            for step, odd in ((outer, 0), (outer, 1), (1 - outer, 0), (1 - outer, 1))]
 
         def far_take(i):
-            take(order[i][0])
+            s, step, odd = order[i]
+            take(s, (1 - outer) * step * odd == 0)
 
         def far_expand(i):
             s = order[i][0]
-            landed(arrived.at[s, 1 - x], recv_side.at[s])
-            expand(s)
+            expand(s, x, lambda: landed(arrived.at[s, 1 - x], recv_side.at[s]))
 
         def far_contract(i):
             s, step, odd = order[i]
@@ -304,15 +335,15 @@
         far_take(0)
         far_take(1)
         weights_ready()
-        relay_down()
         far_expand(0)
         far_take(2)
         far_expand(1)
         far_take(3)
+        relay_down()
         down_ready()
         far_contract(0)
+        far_expand(2)
         far_contract(1)
-        far_expand(2)
         far_expand(3)
         far_contract(2)
         far_contract(3)
@@ -335,13 +366,13 @@
 
         weights_ready()
         near_expand(0)
+        relay_down()
         near_expand(1)
-        relay_down()
+        near_expand(3)
+        near_expand(2)
         down_ready()
         near_contract(0)
         near_contract(1)
-        near_expand(3)
-        near_expand(2)
         near_contract(3)
         near_contract(2)
 
@@ -352,6 +383,7 @@
 
     def finish():
         landed(hidden.at[:, x], send_hid.at[0])
+        shed.wait_send()
         for share in shares:
             share.wait_send()
         relay.wait_send()
@@ -360,7 +392,16 @@
         def _():
             landed(leaving, send_disp.at[0])
             landed(outgoing, send_disp.at[1])
-            landed(arrived.at[:, x], send_side.at[0])
+
+            @pl.when(outer == 0)
+            def _():
+                landed(spare, send_disp.at[2])
+                landed(arrived.at[pl.ds(0, near - 1), x], send_side.at[0])
+
+            @pl.when(outer == 1)
+            def _():
+                landed(arrived.at[:, x], send_side.at[0])
+
             landed(result, send_home.at[0])
 
         @pl.when(c == 0)
@@ -376,7 +417,6 @@
     rows, model = tokens.shape
     capacity = 3 * routes.shape[1] * rows // (2 * n_ep)
     width = gate_weight.shape[2]
-    fpad = round_up(width, 128)
     half, quarter = model // 2, model // 4
     sem = pltpu.SemaphoreType.DMA
     vmem = pl.BlockSpec(memory_space=pltpu.VMEM)
@@ -399,16 +439,17 @@
             pltpu.VMEM((n_ep * capacity, rows), BF16),
             pltpu.VMEM((2, 2, rows, n_ep * capacity // 2), BF16),
             pltpu.VMEM((n_ep // 2, capacity, half), BF16),
+            pltpu.VMEM((capacity, half), BF16),
             pltpu.VMEM((2, 2, capacity, half), BF16),
             pltpu.VMEM((n_ep // 2, 2, capacity, half), BF16),
-            pltpu.VMEM((2, 2, fpad, model), BF16),
-            pltpu.VMEM((2, 2, fpad, half), BF16),
+            pltpu.VMEM((2, 2 * width, model), BF16),
+            pltpu.VMEM((2, 2 * width, half), BF16),
             pltpu.VMEM((width, half), BF16),
-            pltpu.VMEM((n_ep // 2, 2, capacity, 2 * fpad), BF16),
+            pltpu.VMEM((n_ep // 2, 2, capacity, 2 * width), BF16),
             pltpu.VMEM((n_ep // 2, 2, capacity, quarter), BF16),
             pltpu.VMEM((n_ep, capacity, quarter), BF16),
             sem((9,)),
-            sem((2,)), sem((n_ep // 2,)),
+            sem((3,)), sem((n_ep // 2,)),
             sem((1,)), sem((n_ep // 2,)),
             sem((1,)), sem((n_ep // 2,)),
             sem((1,)), sem((3,)),
@@ -419,11 +460,11 @@
     )(*[pltpu.with_memory_space_constraint(operand, pltpu.HBM) for operand in operands])
 
 
-def fits_kernel(n_ep, n_tp, rows, experts, top, model):
+def fits_kernel(n_ep, n_tp, rows, experts, top, model, width):
     capacity = 3 * top * rows // (2 * experts)
     return (
         experts == n_ep and top == 2 and n_ep == 8 and n_tp == 4
-        and capacity % 16 == 0 and rows % 128 == 0 and model % 512 == 0
+        and capacity % 16 == 0 and rows % 128 == 0 and model % 512 == 0 and width % 16 == 0
     )
 
 
@@ -432,7 +473,7 @@
 
     def chosen(*arrays):
         rows, model = arrays[0].shape
-        fits = fits_kernel(n_ep, n_tp, rows, arrays[5].shape[0] * n_ep, arrays[2].shape[1], model)
+        fits = fits_kernel(n_ep, n_tp, rows, arrays[5].shape[0] * n_ep, arrays[2].shape[1], model, arrays[5].shape[2])
         return (fused_body if fits else body)(*arrays)
 
     return jax.shard_map(

time: 28.4 us -> 27 us (0.951)
  the two profiles are of different devices: /device:TPU:0 before, /device:TPU:9 now
where the time goes in v4:
time: 27 us; the launch traced here: 26.9 us
  Pallas kernels  26.2 us (97%)
  local copies, waits for them, and re-layouts  0.66 us (2%)
    pallas_call x1, Pallas kernels, fused_body(): pl.pallas_call(functools.partial(expert_kernel, n_ep, capacity, width), o...  26.2 us
    unnamed x1, local copies, waits for them, and re-layouts  0.66 us

profile of v4, /device:TPU:9, one launch (start us, length us, event | category | flops | bytes accessed | tf_op | source)
XLA Modules:
  0.0 26.9 jit_solution(9275012517167084025)
XLA Ops:
  0.0 26.2 %shard_map.82 = bf16[128,512]{1,0:T(8,128)(2,1)S(1)} custom-call(bf16[128,2048]{1,0:T(8,128)(2,1)} %tokens_hbm.1, f32[1,2048]{1,0:T(1,128)} %bitcast.14, s32[2,128]{1,0:T(2,128)} %bitcast.15, f32[1,128]{1,0:T(1,128)} %bitcast.17, f32[2,128]{1,0:T(2,128)} %bitcast.16, bf16[96,2048]{1,0:T(8,128)(2,1)} %bitcast.11, bf16[96,2048]{1,0:T(8,128)(2,1)} %bitcast.12, ...), custom_call_target="tpu_custom_call" | custom-call | tf_op jit(solution)/shard_map/pallas_call | solution.py:427
  26.2 0.7 %copy.10 = bf16[128,512]{1,0:T(8,128)(2,1)} copy(bf16[128,512]{1,0:T(8,128)(2,1)S(1)} %shard_map.82) | data formatting | bytes 262144

commit v5 on v4

--- a/solution.py
+++ b/solution.py
@@ -98,7 +98,7 @@
     out_ref,
     tokens_ref, gain_ref, routes_ref, prob_ref, logits_ref, normed, select, weigh, leaving, spare, outgoing, arrived, gate_up,
     down_rows, down_other, hidden, result, returned,
-    load_sem, send_disp, recv_disp, send_side, recv_side, send_hid, recv_hid, send_home, recv_home, send_weight, recv_weight,
+    load_sem, send_disp, recv_disp, send_side, recv_side, send_hid, recv_hid, send_home, recv_home, send_weight, recv_weight, ready,
 ):
     loads = [
         pltpu.make_async_copy(source, target, load_sem.at[i])
@@ -122,12 +122,18 @@
     hi, lo = e // 4, (e // 2) % 2
 
     barrier = pltpu.get_barrier_semaphore()
-    for r in reversed(range(n_ep)):
-        for mate in (t, partner):
-            if r or mate is partner:
-                pl.semaphore_signal(
-                    barrier, inc=1, device_id={"ep": toggled(e, r), "tp": mate}, device_id_type=MESH)
-    pl.semaphore_signal(barrier, inc=1, device_id={"ep": e, "tp": across}, device_id_type=MESH)
+
+    def greet(semaphore, ep, tp):
+        pl.semaphore_signal(semaphore, inc=1, device_id={"ep": ep, "tp": tp}, device_id_type=MESH)
+
+    for r in reversed(range(1, n_ep)):
+        greet(barrier, toggled(e, r), t)
+    greet(barrier, e, across)
+
+    @pl.when(c == 1)
+    def _():
+        for r in reversed(range(n_ep)):
+            greet(barrier, toggled(e, r), partner)
 
     def columns(side):
         return pl.ds(pl.multiple_of(side * half, half), half)
@@ -167,23 +173,32 @@
     scale = lax.rsqrt(jnp.mean(values * values, -1, keepdims=True) + 1e-06)
     normed[...] = (values * scale * gain_ref[...]).astype(BF16)
 
-    def packed(begin, end, lanes):
+    def packed(begin, end, q):
+        lanes = pl.ds(pl.multiple_of(q * quarter, quarter), quarter)
         return jnp.dot(
             select[begin * capacity:end * capacity], normed[:, lanes], preferred_element_type=F32
-        ).astype(BF16).reshape(end - begin, capacity, half)
-
-    @pl.when(c == 1)
-    def _():
-        leaving[...] = packed(near, n_ep, columns(x))
+        ).astype(BF16).reshape(end - begin, capacity, quarter)
+
+    @pl.when(c == 1)
+    def _():
+        for q in range(2):
+            leaving[:, q] = packed(near, n_ep, 2 * x + q)
 
     @pl.when(c == 0)
     def _():
-        for side in range(2):
-            both = packed(0, 2, slice(side * half, (side + 1) * half))
-            arrived[0, side] = both[0]
-            outgoing[0, side] = both[1]
-
-    pl.semaphore_wait(barrier, 2 * n_ep)
+        for q in range(4):
+            both = packed(0, 2, q)
+            arrived[0, q] = both[0]
+            outgoing[0, q] = both[1]
+
+    @pl.when(c == 1)
+    def _():
+        pl.semaphore_wait(barrier, n_ep)
+
+    @pl.when(c == 0)
+    def _():
+        pl.semaphore_wait(barrier, 2 * n_ep)
+        greet(ready, e, partner)
 
     def remote(source, target, send, recv, ep, tp):
         return pltpu.make_async_remote_copy(
@@ -193,17 +208,22 @@
     def landed(ref, sem):
         pltpu.make_async_copy(ref, ref, sem).wait()
 
+    own_half, their_half = pl.ds(2 * x, 2), pl.ds(2 - 2 * x, 2)
+
     def far_peer(step, odd):
         return e + flipped(e, 4) + step * flipped(e, 2) + odd * flipped(e, 1)
 
     def send_far(step):
         for odd in range(2):
             s = 2 * step + odd
-            remote(leaving.at[s], arrived.at[s, x], send_disp.at[0], recv_disp.at[s], far_peer(step, odd), t).start()
+            for q in range(2):
+                remote(
+                    leaving.at[s, q], arrived.at[s, 2 * x + q], send_disp.at[0], recv_disp.at[near * q + s],
+                    far_peer(step, odd), t).start()
 
     def pack_near():
-        for side in range(2):
-            outgoing[0:2, side] = packed(2, 4, slice(side * half, (side + 1) * half))
+        for q in range(4):
+            outgoing[0:2, q] = packed(2, 4, q)
 
     first_step = outer
 
@@ -212,19 +232,24 @@
         send_far(first_step)
         send_far(1 - first_step)
 
+    @pl.when(c == 1)
+    def _():
+        pack_near()
+
+    @pl.when(c == 1)
+    def _():
+        pl.semaphore_wait(ready, 1)
+
+    def send_near(s):
+        remote(outgoing.at[s - 2], arrived.at[s], send_disp.at[1], recv_disp.at[s], toggled(e, s), partner).start()
+
+    @pl.when(c == 1)
+    def _():
+
         @pl.when(outer == 0)
         def _():
-            spare[...] = packed(n_ep - 1, n_ep, columns(1 - x))[0]
-            remote(spare, arrived.at[3, 1 - x], send_disp.at[2], recv_side.at[3], far_peer(1, 1), t).start()
-
-    @pl.when(c == 1)
-    def _():
-        pack_near()
-
-    @pl.when(c == 1)
-    def _():
-        for s in (3, 2):
-            remote(outgoing.at[s - 2], arrived.at[s], send_disp.at[1], recv_disp.at[s], toggled(e, s), partner).start()
+            send_near(3)
+            send_near(2)
 
     @pl.when(c == 0)
     def _():
@@ -260,16 +285,13 @@
         return lax.dot_general(left, right, (((1,), (1,)), ((), ())), preferred_element_type=F32)
 
     def take(s, on=True):
-        mine = arrived.at[s, x]
-        landed(mine, recv_disp.at[s])
-
-        def pass_on():
-            remote(mine, mine, send_side.at[0], recv_side.at[s], e, across).start()
-
-        if on is True:
-            pass_on()
-        else:
-            pl.when(on)(pass_on)
+        for q in range(2):
+            mine = arrived.at[s, 2 * x + q]
+            landed(mine, recv_disp.at[near * q + s])
+
+            @pl.when(on)
+            def _():
+                remote(mine, mine, send_side.at[0], recv_side.at[s], e, across).start()
 
     def expand(s, begin=0, wait=None):
         gate = jnp.zeros((capacity, 2 * width), F32)
@@ -278,7 +300,7 @@
             if wait is not None and side is not begin:
                 wait()
             for q in range(2):
-                part = arrived[s, side, :, q * quarter:(q + 1) * quarter]
+                part = arrived[s, 2 * side + q]
                 lanes = pl.ds(pl.multiple_of(side * half + q * quarter, quarter), quarter)
                 gate = gate + product(part, gate_up[0, :, lanes])
                 up = up + product(part, gate_up[1, :, lanes])
@@ -321,11 +343,11 @@
 
         def far_take(i):
             s, step, odd = order[i]
-            take(s, (1 - outer) * step * odd == 0)
+            take(s)
 
         def far_expand(i):
             s = order[i][0]
-            expand(s, x, lambda: landed(arrived.at[s, 1 - x], recv_side.at[s]))
+            expand(s, x, lambda: landed(arrived.at[s, their_half], recv_side.at[s]))
 
         def far_contract(i):
             s, step, odd = order[i]
@@ -334,6 +356,12 @@
 
         far_take(0)
         far_take(1)
+
+        @pl.when(outer == 1)
+        def _():
+            send_near(3)
+            send_near(2)
+
         weights_ready()
         far_expand(0)
         far_take(2)
@@ -393,15 +421,7 @@
             landed(leaving, send_disp.at[0])
             landed(outgoing, send_disp.at[1])
 
-            @pl.when(outer == 0)
-            def _():
-                landed(spare, send_disp.at[2])
-                landed(arrived.at[pl.ds(0, near - 1), x], send_side.at[0])
-
-            @pl.when(outer == 1)
-            def _():
-                landed(arrived.at[:, x], send_side.at[0])
-
+            landed(arrived.at[:, own_half], send_side.at[0])
             landed(result, send_home.at[0])
 
         @pl.when(c == 0)
@@ -438,10 +458,10 @@
             pltpu.VMEM((rows, model), BF16),
             pltpu.VMEM((n_ep * capacity, rows), BF16),
             pltpu.VMEM((2, 2, rows, n_ep * capacity // 2), BF16),
-            pltpu.VMEM((n_ep // 2, capacity, half), BF16),
-            pltpu.VMEM((capacity, half), BF16),
-            pltpu.VMEM((2, 2, capacity, half), BF16),
-            pltpu.VMEM((n_ep // 2, 2, capacity, half), BF16),
+            pltpu.VMEM((n_ep // 2, 2, capacity, quarter), BF16),
+            pltpu.VMEM((2, capacity, quarter), BF16),
+            pltpu.VMEM((2, 4, capacity, quarter), BF16),
+            pltpu.VMEM((n_ep // 2, 4, capacity, quarter), BF16),
             pltpu.VMEM((2, 2 * width, model), BF16),
             pltpu.VMEM((2, 2 * width, half), BF16),
             pltpu.VMEM((width, half), BF16),
@@ -449,11 +469,11 @@
             pltpu.VMEM((n_ep // 2, 2, capacity, quarter), BF16),
             pltpu.VMEM((n_ep, capacity, quarter), BF16),
             sem((9,)),
-            sem((3,)), sem((n_ep // 2,)),
+            sem((2,)), sem((n_ep,)),
             sem((1,)), sem((n_ep // 2,)),
             sem((1,)), sem((n_ep // 2,)),
             sem((1,)), sem((3,)),
-            sem((5,)), sem((5,)),
+            sem((5,)), sem((5,)), pltpu.SemaphoreType.REGULAR,
         ],
         compiler_params=pltpu.CompilerParams(
             collective_id=0, has_side_effects=True, vmem_limit_bytes=32 * 1024 * 1024),

time: 27 us -> 26.5 us (0.981)
  the two profiles are of different devices: /device:TPU:9 before, /device:TPU:0 now
where the time goes in v5:
time: 26.5 us; the launch traced here: 26.2 us
  Pallas kernels  25.5 us (96%)
  local copies, waits for them, and re-layouts  0.66 us (2%)
    pallas_call x1, Pallas kernels, fused_body(): pl.pallas_call(functools.partial(expert_kernel, n_ep, capacity, width), o...  25.5 us
    unnamed x1, local copies, waits for them, and re-layouts  0.66 us

profile of v5, /device:TPU:0, one launch (start us, length us, event | category | flops | bytes accessed | tf_op | source)
XLA Modules:
  0.0 26.2 jit_solution(6329076142723220664)
XLA Ops:
  0.0 25.5 %shard_map.82 = bf16[128,512]{1,0:T(8,128)(2,1)S(1)} custom-call(bf16[128,2048]{1,0:T(8,128)(2,1)} %tokens_hbm.1, f32[1,2048]{1,0:T(1,128)} %bitcast.14, s32[2,128]{1,0:T(2,128)} %bitcast.15, f32[1,128]{1,0:T(1,128)} %bitcast.17, f32[2,128]{1,0:T(2,128)} %bitcast.16, bf16[96,2048]{1,0:T(8,128)(2,1)} %bitcast.11, bf16[96,2048]{1,0:T(8,128)(2,1)} %bitcast.12, ...), custom_call_target="tpu_custom_call" | custom-call | tf_op jit(solution)/shard_map/pallas_call | solution.py:447
  25.5 0.7 %copy.10 = bf16[128,512]{1,0:T(8,128)(2,1)} copy(bf16[128,512]{1,0:T(8,128)(2,1)S(1)} %shard_map.82) | data formatting | bytes 262144

commit v6 on v5

--- a/solution.py
+++ b/solution.py
@@ -255,9 +255,18 @@
     def _():
         remote(outgoing.at[0], arrived.at[1], send_disp.at[0], recv_disp.at[1], toggled(e, 1), t).start()
 
-    shed = remote(down_other, owned(down_rows, x, c), send_weight.at[0], recv_weight.at[0], e, across)
+    def down_part(begin, size):
+        return remote(
+            down_other.at[pl.ds(begin, size)], owned(down_rows, x, c).at[pl.ds(begin, size)], send_weight.at[0], recv_weight.at[0], e, across)
+
+    cut = width // 2 // 16 * 16
+    late = c == 1
     fetches[0].wait()
-    shed.start()
+    down_part(0, cut).start()
+
+    @pl.when(jnp.logical_not(late))
+    def _():
+        down_part(cut, width - cut).start()
 
     shares = [
         remote(owned(gate_up, 0, c), owned(gate_up, 0, c), send_weight.at[1], recv_weight.at[1], e, partner),
@@ -361,6 +370,11 @@
         def _():
             send_near(3)
             send_near(2)
+
+
+        @pl.when(late)
+        def _():
+            down_part(cut, width - cut).start()
 
         weights_ready()
         far_expand(0)
@@ -411,7 +425,7 @@
 
     def finish():
         landed(hidden.at[:, x], send_hid.at[0])
-        shed.wait_send()
+        landed(down_other, send_weight.at[0])
         for share in shares:
             share.wait_send()
         relay.wait_send()

time: 26.5 us -> 26.3 us (level)
  Pallas kernels: 25.5 us -> 25.2 us
    pallas_call x1, Pallas kernels: 25.5 us -> 25.2 us  [fused_body(): pl.pallas_call(functools.partial(expert_kernel, n_ep, capacity, width), o...]
where the time goes in v6:
time: 26.3 us; the launch traced here: 25.8 us
  Pallas kernels  25.2 us (96%)
  local copies, waits for them, and re-layouts  0.66 us (3%)
    pallas_call x1, Pallas kernels, fused_body(): pl.pallas_call(functools.partial(expert_kernel, n_ep, capacity, width), o...  25.2 us
    unnamed x1, local copies, waits for them, and re-layouts  0.66 us

profile of v6, /device:TPU:0, one launch (start us, length us, event | category | flops | bytes accessed | tf_op | source)
XLA Modules:
  0.0 25.8 jit_solution(15065620191116298382)
XLA Ops:
  0.0 25.2 %shard_map.82 = bf16[128,512]{1,0:T(8,128)(2,1)S(1)} custom-call(bf16[128,2048]{1,0:T(8,128)(2,1)} %tokens_hbm.1, f32[1,2048]{1,0:T(1,128)} %bitcast.14, s32[2,128]{1,0:T(2,128)} %bitcast.15, f32[1,128]{1,0:T(1,128)} %bitcast.17, f32[2,128]{1,0:T(2,128)} %bitcast.16, bf16[96,2048]{1,0:T(8,128)(2,1)} %bitcast.11, bf16[96,2048]{1,0:T(8,128)(2,1)} %bitcast.12, ...), custom_call_target="tpu_custom_call" | custom-call | tf_op jit(solution)/shard_map/pallas_call | solution.py:461
  25.2 0.7 %copy.10 = bf16[128,512]{1,0:T(8,128)(2,1)} copy(bf16[128,512]{1,0:T(8,128)(2,1)S(1)} %shard_map.82) | data formatting | bytes 262144

commit v7 on v6

--- a/solution.py
+++ b/solution.py
@@ -141,6 +141,9 @@
     def owned(ref, side, core):
         return ref.at[side, pl.ds(pl.multiple_of(core * width, width), width)]
 
+    def both(ref, core):
+        return ref.at[:, pl.ds(pl.multiple_of(core * width, width), width)]
+
     fetches = [
         pltpu.make_async_copy(down_ref.at[:, columns(1 - x)], down_other, load_sem.at[5]),
         pltpu.make_async_copy(gate_ref, owned(gate_up, 0, c), load_sem.at[6]),
@@ -270,14 +273,14 @@
 
     shares = [
         remote(owned(gate_up, 0, c), owned(gate_up, 0, c), send_weight.at[1], recv_weight.at[1], e, partner),
-        remote(owned(gate_up, 1, c), owned(gate_up, 1, c), send_weight.at[2], recv_weight.at[2], e, partner),
-        remote(owned(down_rows, x, c), owned(down_rows, x, c), send_weight.at[3], recv_weight.at[3], e, partner),
+        remote(owned(gate_up, 1, c), owned(gate_up, 1, c), send_weight.at[1], recv_weight.at[1], e, partner),
+        remote(owned(down_rows, x, c), owned(down_rows, x, c), send_weight.at[0], recv_weight.at[2], e, partner),
     ]
     for fetch, share in zip(fetches[1:], shares):
         fetch.wait()
         share.start()
     far_rows = owned(down_rows, 1 - x, c)
-    relay = remote(far_rows, far_rows, send_weight.at[4], recv_weight.at[4], e, partner)
+    relay = remote(far_rows, far_rows, send_weight.at[0], recv_weight.at[2], e, partner)
 
     logit0, logit1 = logits_ref[0:1, :], logits_ref[1:2, :]
     top = jnp.maximum(logit0, logit1)
@@ -328,16 +331,14 @@
             remote(result.at[s, j], returned.at[r], send_home.at[0], recv_home.at[group], peer, 2 * x + j).start()
 
     def weights_ready():
-        for kind in range(2):
-            landed(owned(gate_up, kind, 1 - c), recv_weight.at[1 + kind])
+        landed(both(gate_up, 1 - c), recv_weight.at[1])
 
     def relay_down():
         landed(far_rows, recv_weight.at[0])
         relay.start()
 
     def down_ready():
-        landed(owned(down_rows, x, 1 - c), recv_weight.at[3])
-        landed(owned(down_rows, 1 - x, 1 - c), recv_weight.at[4])
+        landed(both(down_rows, 1 - c), recv_weight.at[2])
 
     def merge(part):
         back = returned[part * near:(part + 1) * near].reshape(slots // 2, quarter)
@@ -425,10 +426,8 @@
 
     def finish():
         landed(hidden.at[:, x], send_hid.at[0])
-        landed(down_other, send_weight.at[0])
-        for share in shares:
-            share.wait_send()
-        relay.wait_send()
+        landed(down_rows.at[:, pl.ds(0, 3 * width // 2)], send_weight.at[0])
+        landed(both(gate_up, c), send_weight.at[1])
 
         @pl.when(c == 1)
         def _():
@@ -487,7 +486,7 @@
             sem((1,)), sem((n_ep // 2,)),
             sem((1,)), sem((n_ep // 2,)),
             sem((1,)), sem((3,)),
-            sem((5,)), sem((5,)), pltpu.SemaphoreType.REGULAR,
+            sem((2,)), sem((3,)), pltpu.SemaphoreType.REGULAR,
         ],
         compiler_params=pltpu.CompilerParams(
             collective_id=0, has_side_effects=True, vmem_limit_bytes=32 * 1024 * 1024),
@@ -498,7 +497,7 @@
     capacity = 3 * top * rows // (2 * experts)
     return (
         experts == n_ep and top == 2 and n_ep == 8 and n_tp == 4
-        and capacity % 16 == 0 and rows % 128 == 0 and model % 512 == 0 and width % 16 == 0
+        and capacity % 16 == 0 and rows % 128 == 0 and model % 512 == 0 and width % 32 == 0
     )
 
 

time: 26.3 us -> 26.3 us (level)
  no operation moved by 1% of the time
where the time goes in v7:
time: 26.3 us; the launch traced here: 25.8 us
  Pallas kernels  25.1 us (95%)
  local copies, waits for them, and re-layouts  0.66 us (3%)
    pallas_call x1, Pallas kernels, fused_body(): pl.pallas_call(functools.partial(expert_kernel, n_ep, capacity, width), o...  25.1 us
    unnamed x1, local copies, waits for them, and re-layouts  0.66 us

profile of v7, /device:TPU:0, one launch (start us, length us, event | category | flops | bytes accessed | tf_op | source)
XLA Modules:
  0.0 25.8 jit_solution(5218929692047357207)
XLA Ops:
  0.0 25.1 %shard_map.82 = bf16[128,512]{1,0:T(8,128)(2,1)S(1)} custom-call(bf16[128,2048]{1,0:T(8,128)(2,1)} %tokens_hbm.1, f32[1,2048]{1,0:T(1,128)} %bitcast.14, s32[2,128]{1,0:T(2,128)} %bitcast.15, f32[1,128]{1,0:T(1,128)} %bitcast.17, f32[2,128]{1,0:T(2,128)} %bitcast.16, bf16[96,2048]{1,0:T(8,128)(2,1)} %bitcast.11, bf16[96,2048]{1,0:T(8,128)(2,1)} %bitcast.12, ...), custom_call_target="tpu_custom_call" | custom-call | tf_op jit(solution)/shard_map/pallas_call | solution.py:460
  25.1 0.7 %copy.10 = bf16[128,512]{1,0:T(8,128)(2,1)} copy(bf16[128,512]{1,0:T(8,128)(2,1)S(1)} %shard_map.82) | data formatting | bytes 262144
